TPU v7x, 256 devices: a whole 4x4x8 slice. The times are simulated.
256 devices in a mesh: sp: 64 (over z, y, core), tp: 4 (over x).
Axes of the slice: x: 4, y: 4, z: 8, core: 2. Of those that a mesh axis runs over, the one named last changes fastest.
Arguments:
- conv_outer: bfloat16 [49152, 2048], P('sp', 'tp'), may hold values from -6 to 6
- conv_inner: bfloat16 [49152, 2048], P('sp', 'tp'), may hold values from -6 to 6
- conv_input: bfloat16 [49152, 2048], P('sp', 'tp'), may hold values from -6 to 6
- conv_taps: float32 [3, 2048], P(None, 'tp'), may hold values from -3.5 to 3.5
- out_weight: bfloat16 [2048, 2048], P('tp'), may hold values from -0.125 to 0.125
- mix_gate: bfloat16 [49152, 2048], P(('sp', 'tp')), may hold values from -8 to 8
- residual: bfloat16 [49152, 2048], P(('sp', 'tp')), may hold values from -6 to 6
- mix_gain: float32 [2048], replicated, may hold values from 0.1 to 1.9
- expert_gain: float32 [2048], replicated, may hold values from 0.1 to 1.9
- expert_ids: int32 [49152, 2], P(('sp', 'tp')), may hold values from 0 to 63, all different within a row; in each aligned block of 192 rows (0 to 191, 192 to 383, ...) at most 12 rows name the same one
- group_share: float32 [49152], P(('sp', 'tp')), may hold values from 0.25 to 1
- pair_scores: float32 [49152, 2], P(('sp', 'tp')), may hold values from -8 to 8
- gate_experts: bfloat16 [64, 2048, 512], P('sp'), may hold values from -0.125 to 0.125
- up_experts: bfloat16 [64, 2048, 512], P('sp'), may hold values from -0.125 to 0.125
- down_experts: bfloat16 [64, 512, 2048], P('sp'), may hold values from -0.25 to 0.25
Outputs:
- layer_out: bfloat16 [49152, 2048], P(('sp', 'tp'))
Inputs may be any that keep to these rules, and one draw needn't show every extreme that they name: `expert_ids`: within the rows of one device (aligned blocks of 192 rows), no expert is named by more than 12 rows, a bound that some block reaches; the 2 experts of a row differ.
All inputs are finite; a program needn't handle non-finite values.
Results may differ from a plain program's by a relative error of at most 0.0069.
Values may be sent and summed in bfloat16 or wider, within the bound.
A program may use at most 128 MiB of HBM per device.

v0:
```python
import jax
import jax.numpy as jnp
from jax import lax
from jax.sharding import Mesh
from jax.sharding import PartitionSpec as P

SP = ("sp_0", "sp_1", "sp_2")
SP_TP = ("sp_0", "sp_1", "sp_2", "tp")


epsilon = 1e-06


def passed_along(value, axis, steps):
    count = lax.axis_size(axis)
    leading, last = (max(0, -steps), min(count, count - steps))
    return lax.ppermute(value, axis, [(source, source + steps) for source in range(leading, last)])


def split_up(value, dim, peers):
    before, after = (value.shape[:dim], value.shape[dim + 1 :])
    return jnp.moveaxis(value.reshape(*before, peers, -1, *after), dim, 0)


def sent_and_summed(value, axis, dim):
    peers = lax.axis_size(axis)
    parts = lax.all_to_all(split_up(value, dim, peers), axis, 0, 0, tiled=True)
    return jnp.sum(parts.astype(jnp.float32), axis=0)


def joined_along(parts, dim):
    dims = list(parts.shape[1:])
    dims[dim] *= parts.shape[0]
    return jnp.moveaxis(parts, 0, dim).reshape(dims)


def turned_blocks(parts, axes, turns):
    inside = parts.shape[1:]
    out = parts.reshape(*(lax.axis_size(a) for a in axes), *inside)
    for k in turns:
        out = lax.all_to_all(out, axes[k], k, k, tiled=True)
    return out.reshape(-1, *inside)


def two_step_exchange(value, groups, turns, split_dim, concat_dim):
    peers = lax.axis_size(groups[0]) * lax.axis_size(groups[1])
    parts = split_up(value, split_dim, peers)
    return joined_along(turned_blocks(parts, groups, turns), concat_dim)


def rms_scale(values, gain):
    return values * lax.rsqrt(jnp.mean(values * values, axis=-1, keepdims=True) + epsilon) * gain


def per_device(
    conv_outer,
    conv_inner,
    conv_input,
    conv_taps,
    out_weight,
    mix_gate,
    residual,
    mix_gain,
    expert_gain,
    expert_ids,
    group_share,
    pair_scores,
    gate_experts,
    up_experts,
    down_experts,
):
    kept = conv_taps.shape[0] - 1
    earlier = passed_along((conv_inner[-kept:], conv_input[-kept:]), SP, 1)
    inner = jnp.concatenate(
        [
            earlier[0].astype(jnp.float32) * earlier[1].astype(jnp.float32),
            conv_inner.astype(jnp.float32) * conv_input.astype(jnp.float32),
        ],
        0,
    )
    length = conv_inner.shape[0]
    conv = conv_taps[0] * inner[0:length]
    for offset in range(1, kept + 1):
        conv = conv + conv_taps[offset] * inner[offset : offset + length]
    mixed_rows = (conv_outer.astype(jnp.float32) * conv).astype(jnp.bfloat16)
    own_rows = residual.shape[0]
    projected = sent_and_summed(
        jnp.dot(mixed_rows, out_weight, preferred_element_type=jnp.float32).astype(jnp.bfloat16),
        "tp",
        0,
    )
    mixed = jax.nn.sigmoid(mix_gate.astype(jnp.float32)) * projected
    hidden_state = (residual.astype(jnp.float32) + rms_scale(mixed, mix_gain)).astype(jnp.bfloat16)
    normed = rms_scale(hidden_state.astype(jnp.float32), expert_gain).astype(jnp.bfloat16)
    experts_all = lax.axis_size(SP) * gate_experts.shape[0]
    per_token = expert_ids.shape[1]
    capacity = 2 * per_token * own_rows // experts_all
    expert_of = expert_ids.reshape(-1)
    count = expert_of.shape[0]
    onehot = (expert_of[:, None] == jnp.arange(experts_all, dtype=jnp.int32)[None, :]).astype(
        jnp.int32
    )
    ranks = jnp.sum((jnp.cumsum(onehot, axis=0) - 1) * onehot, axis=1)
    slot_of = expert_of * capacity + ranks
    matched = slot_of[None, :] == jnp.arange(experts_all * capacity, dtype=jnp.int32)[:, None]
    source_of = jnp.sum(jnp.where(matched, jnp.arange(count, dtype=jnp.int32)[None, :], 0), axis=1)
    filled = jnp.any(matched, axis=1)
    outgoing = jnp.where(
        filled[:, None], normed[source_of // per_token], jnp.zeros((), jnp.bfloat16)
    )
    outgoing = outgoing.reshape(experts_all, capacity, normed.shape[1])
    arrived = two_step_exchange(outgoing, (("sp_0", "sp_1"), "sp_2"), (0, 1), 0, 0)
    layout = arrived.shape
    rows = arrived.reshape(-1, layout[2])
    first = jnp.dot(rows, gate_experts[0], preferred_element_type=jnp.float32)
    second = jnp.dot(rows, up_experts[0], preferred_element_type=jnp.float32)
    inner_hidden = (jax.nn.silu(first) * second).astype(jnp.bfloat16)
    result = jnp.dot(inner_hidden, down_experts[0], preferred_element_type=jnp.float32).astype(
        jnp.bfloat16
    )
    served = result.reshape(layout[0], layout[1], -1)
    returned = lax.all_to_all(served, SP, split_axis=0, concat_axis=0, tiled=True)
    picked = returned.reshape(experts_all * capacity, -1)[slot_of].reshape(own_rows, per_token, -1)
    weights = group_share[:, None] * jax.nn.softmax(pair_scores, axis=-1)
    result = hidden_state.astype(jnp.float32)
    for slot in range(per_token):
        result = result + weights[:, slot : slot + 1] * picked[:, slot].astype(jnp.float32)
    return result.astype(jnp.bfloat16)


def solution(mesh):
    torus = Mesh(mesh.devices.reshape(8, 4, 2, mesh.shape["tp"]), ("sp_0", "sp_1", "sp_2", "tp"))
    return jax.shard_map(
        per_device,
        mesh=torus,
        in_specs=(
            P(SP, "tp"),
            P(SP, "tp"),
            P(SP, "tp"),
            P(None, "tp"),
            P("tp", None),
            P(SP_TP, None),
            P(SP_TP, None),
            P(),
            P(),
            P(SP_TP, None),
            P(SP_TP),
            P(SP_TP, None),
            P(SP, None, None),
            P(SP, None, None),
            P(SP, None, None),
        ),
        out_specs=P(SP_TP, None),
        check_vma=False,
    )
```

profile of v0, /device:TPU:1, one launch (start us, length us, event | category | flops | bytes accessed | tf_op | source)
XLA Modules:
  0.0 310.8 jit_solution(6901631333870964487)
XLA Ops:
  0.0 0.9 slice.40
  0.9 4.6 %collective-permute-start = (bf16[2,512]{1,0:T(2,128)(2,1)S(1)}, bf16[2,512]{1,0:T(2,128)(2,1)S(1)}, u32[]{:S(2)}, u32[]{:S(2)}) collective-permute-start(bf16[2,512]{1,0:T(2,128)(2,1)S(1)} %slice.40), channel_id=1, source_target_pairs={{0,4},{4,8},{8,12},{12,16},{16,20},{20,24},{24,28},{28,32},{32,36}... | collective-permute-start | bytes 6152 | tf_op jit(solution)/shard_map/ppermute | solution.py:17
  5.4 0.7 slice.41
  6.1 2.0 collective-permute-start.1
  8.2 1.6 convert_multiply_fusion.4
  9.8 0.0 collective-permute-done.1
  9.9 3.7 %convolution_convert_fusion.1 = bf16[768,2048]{1,0:T(8,128)(2,1)} fusion(bf16[512,2048]{1,0:T(8,128)(2,1)S(1)} %copy-done, f32[2,512]{1,0:T(2,128)S(1)} %convert_multiply_fusion.5, f32[768,512]{1,0:T(8,128)S(1)} %convert_multiply_fusion.4, bf16[768,512]{1,0:T(8,128)(2,1)S(1)} %copy-done.12, f32[512]{0:T(512)S(1)} %bitcast.55, f32[512]{0:T(512)S(1)} %bitcast.56, ...), kind=kOutput, calls=%fused_computation.5 | convolution fusion | flops 1616117760 | bytes 7612416 | tf_op jit(solution)/shard_map/dot_general | solution.py:88
  13.6 4.1 %all-to-all-start = ((bf16[4,192,2048]{2,1,0:T(8,128)(2,1)}), bf16[4,192,2048]{2,1,0:T(8,128)(2,1)S(1)}, u32[]{:S(2)}, u32[]{:S(2)}) async-start(bf16[4,192,2048]{2,1,0:T(8,128)(2,1)} %bitcast.50), calls=%async_computation | async-start | bytes 6291456 | tf_op jit(solution)/shard_map/all_to_all | solution.py:27
  17.7 0.1 copy.31
  17.8 0.1 eq.39
  18.0 0.1 reshape.172
  18.1 0.9 reduce-window.6
  19.1 0.2 slice_reduce_fusion
  19.3 0.1 fusion.27
  19.4 0.2 fusion.19
  19.6 0.1 broadcast_in_dim.26
  19.8 0.2 select_reduce_fusion
  20.0 34.6 %all-to-all-done = bf16[4,192,2048]{2,1,0:T(8,128)(2,1)S(1)} async-done(((bf16[4,192,2048]{2,1,0:T(8,128)(2,1)}), bf16[4,192,2048]{2,1,0:T(8,128)(2,1)S(1)}, u32[]{:S(2)}, u32[]{:S(2)}) %all-to-all-start) | async-done | bytes 3145760 | tf_op jit(solution)/shard_map/all_to_all | solution.py:27
  54.6 0.6 convert_reduce_fusion
  55.2 0.5 copy-done.4
  55.7 0.5 multiply_reduce_fusion
  56.3 0.6 copy-done.5
  56.9 0.8 fusion.11
  57.7 0.9 copy-done.2
  58.5 0.3 fusion.13
  58.8 4.3 %gather_fusion = bf16[768,2048]{1,0:T(8,128)(2,1)} fusion(bf16[192,2048]{1,0:T(8,128)(2,1)S(1)} %fusion.13, s32[1024]{0:T(1024)S(1)} %pad_clamp_fusion.1), kind=kCustom, calls=%fused_computation | custom fusion | bytes 6294528 | tf_op jit(solution)/shard_map/gather | solution.py:109
  63.1 6.1 %gather.9 = bf16[32,2,1,12,2048]{4,3,1,0,2:T(8,128)(2,1)} reshape(bf16[768,2048]{1,0:T(8,128)(2,1)} %gather_fusion) | data formatting | bytes 6291456 | tf_op jit(solution)/shard_map/gather | solution.py:109
  69.1 2.5 broadcast_select_fusion
  71.7 3.3 %copy.34 = bf16[32,2,1,12,2048]{4,1,3,2,0:T(2,128)(2,1)S(1)} copy(bf16[32,2,1,12,2048]{4,3,1,0,2:T(8,128)(2,1)S(1)} %broadcast_select_fusion) | data formatting | bytes 6291456 | tf_op jit(solution)/shard_map/jit(_where)/select_n | solution.py:108
  75.0 81.3 %all_to_all.20 = bf16[32,2,1,12,2048]{4,1,3,2,0:T(2,128)(2,1)S(1)} all-to-all(bf16[32,2,1,12,2048]{4,1,3,2,0:T(2,128)(2,1)S(1)} %copy.34), channel_id=1, replica_groups=mesh['sp_0'=8,'sp_1'=4,'sp_2'=2,'tp'=4] {'sp_0','sp_1'}, dimensions={0} | all-to-all | bytes 6291456 | tf_op jit(solution)/shard_map/all_to_all | solution.py:41
  156.2 1.7 copy.35
  158.0 9.3 %all_to_all.21 = bf16[32,2,1,12,2048]{4,0,3,2,1:T(8,128)(2,1)S(1)} all-to-all(bf16[32,2,1,12,2048]{4,0,3,2,1:T(8,128)(2,1)S(1)} %copy.35), channel_id=1, replica_groups=mesh['sp_0'=8,'sp_1'=4,'sp_2'=2,'tp'=4] {'sp_2'}, dimensions={1} | all-to-all | bytes 6291456 | tf_op jit(solution)/shard_map/all_to_all | solution.py:41
  167.2 3.7 %copy.36 = bf16[32,2,1,12,2048]{4,3,1,0,2:T(8,128)(2,1)} copy(bf16[32,2,1,12,2048]{4,0,3,2,1:T(8,128)(2,1)S(1)} %all_to_all.21) | data formatting | bytes 6291456 | tf_op jit(solution)/shard_map/all_to_all | solution.py:41
  170.9 4.7 %reshape_reshape_reshape.4 = bf16[768,2048]{1,0:T(8,128)(2,1)S(1)} reshape(bf16[32,2,1,12,2048]{4,3,1,0,2:T(8,128)(2,1)} %copy.36) | data formatting | bytes 6291456 | tf_op jit(solution)/shard_map/reshape;reshape;reshape | solution.py:114
  175.6 4.5 %fusion.3 = f32[768,512]{1,0:T(8,128)} fusion(bf16[768,2048]{1,0:T(8,128)(2,1)S(1)} %reshape_reshape_reshape.4, bf16[1,2048,512]{2,1,0:T(8,128)(2,1)} %param.27), kind=kOutput, calls=%fused_computation.12 | convolution fusion | flops 1610612736 | bytes 6815744 | tf_op jit(solution)/shard_map/dot_general | solution.py:115
  180.2 7.9 %convolution_convert_fusion = bf16[768,2048]{1,0:T(8,128)(2,1)} fusion(bf16[1,512,2048]{2,1,0:T(8,128)(2,1)} %param.29, f32[768,512]{1,0:T(8,128)} %fusion.3, bf16[768,2048]{1,0:T(8,128)(2,1)S(1)} %reshape_reshape_reshape.4, bf16[1,2048,512]{2,1,0:T(8,128)(2,1)} %param.28), kind=kOutput, calls=%fused_computation.4 | convolution fusion | flops 3225157632 | bytes 12058624 | tf_op jit(solution)/shard_map/dot_general | solution.py:118
  188.1 6.1 %reshape.174 = bf16[64,12,2048]{2,1,0:T(8,128)(2,1)} reshape(bf16[768,2048]{1,0:T(8,128)(2,1)} %convolution_convert_fusion) | data formatting | bytes 6291456 | tf_op jit(solution)/shard_map/reshape | solution.py:121
  194.1 6.4 %all-to-all-start.3 = ((bf16[64,12,2048]{2,1,0:T(8,128)(2,1)}), bf16[64,12,2048]{2,1,0:T(8,128)(2,1)}, u32[]{:S(2)}, u32[]{:S(2)}) async-start(bf16[64,12,2048]{2,1,0:T(8,128)(2,1)} %reshape.174), calls=%async_computation.3 | async-start | bytes 8388608 | tf_op jit(solution)/shard_map/all_to_all | solution.py:122
  200.6 0.1 copy.37
  200.7 0.1 mul.176
  201.0 94.3 %all-to-all-done.3 = bf16[64,12,2048]{2,1,0:T(8,128)(2,1)} async-done(((bf16[64,12,2048]{2,1,0:T(8,128)(2,1)}), bf16[64,12,2048]{2,1,0:T(8,128)(2,1)}, u32[]{:S(2)}, u32[]{:S(2)}) %all-to-all-start.3) | async-done | bytes 3145760 | tf_op jit(solution)/shard_map/all_to_all | solution.py:122
  295.3 4.7 %reshape.175 = bf16[768,2048]{1,0:T(8,128)(2,1)S(1)} reshape(bf16[64,12,2048]{2,1,0:T(8,128)(2,1)} %all-to-all-done.3) | data formatting | bytes 6291456 | tf_op jit(solution)/shard_map/reshape | solution.py:123
  300.0 3.1 %gather_fusion.1 = bf16[384,2048]{1,0:T(8,128)(2,1)} fusion(bf16[768,2048]{1,0:T(8,128)(2,1)S(1)} %reshape.175, s32[1024]{0:T(1024)S(1)} %pad_clamp_fusion), kind=kCustom, calls=%fused_computation.1 | custom fusion | bytes 3147264 | tf_op jit(solution)/shard_map/gather | solution.py:123
  303.2 2.8 reshape.176
  305.9 0.0 copy-start.3
  306.0 2.2 fusion.34
  308.2 0.0 copy-start.1
  308.2 2.6 fusion.15
  (38 shorter events, 0.3 us)
Async XLA Ops:
  0.0 9.9 %copy-start = (bf16[512,2048]{1,0:T(8,128)(2,1)S(1)}, bf16[512,2048]{1,0:T(8,128)(2,1)}, u32[]{:S(2)}) copy-start(bf16[512,2048]{1,0:T(8,128)(2,1)} %param.19) | copy-start | bytes 6291460
  0.9 9.0 %collective-permute-start = (bf16[2,512]{1,0:T(2,128)(2,1)S(1)}, bf16[2,512]{1,0:T(2,128)(2,1)S(1)}, u32[]{:S(2)}, u32[]{:S(2)}) collective-permute-start(bf16[2,512]{1,0:T(2,128)(2,1)S(1)} %slice.40), channel_id=1, source_target_pairs={{0,4},{4,8},{8,12},{12,16},{16,20},{20,24},{24,28},{28,32},{32,36}... | collective-permute-start | bytes 6152 | tf_op jit(solution)/shard_map/ppermute | solution.py:17
  6.1 3.7 %copy-start.10 = (f32[3,512]{1,0:T(4,128)S(1)}, f32[3,512]{1,0:T(4,128)}, u32[]{:S(2)}) copy-start(f32[3,512]{1,0:T(4,128)} %param.18) | copy-start | bytes 18436
  6.1 3.7 %copy-start.12 = (bf16[768,512]{1,0:T(8,128)(2,1)S(1)}, bf16[768,512]{1,0:T(8,128)(2,1)}, u32[]{:S(2)}) copy-start(bf16[768,512]{1,0:T(8,128)(2,1)} %param.15) | copy-start | bytes 2359300
  6.1 3.7 %collective-permute-start.1 = (bf16[2,512]{1,0:T(2,128)(2,1)S(1)}, bf16[2,512]{1,0:T(2,128)(2,1)S(1)}, u32[]{:S(2)}, u32[]{:S(2)}) collective-permute-start(bf16[2,512]{1,0:T(2,128)(2,1)S(1)} %slice.41), channel_id=1, source_target_pairs={{0,4},{4,8},{8,12},{12,16},{16,20},{20,24},{24,28},{28,32},{32,36}... | collective-permute-start | bytes 6152 | tf_op jit(solution)/shard_map/ppermute | solution.py:17
  13.6 4.2 %copy-start.9 = (s32[192,2]{0,1:T(2,128)S(1)}, s32[192,2]{0,1:T(2,128)}, u32[]{:S(2)}) copy-start(s32[192,2]{0,1:T(2,128)} %param.24) | copy-start | bytes 4612
  13.6 41.0 %all-to-all-start = ((bf16[4,192,2048]{2,1,0:T(8,128)(2,1)}), bf16[4,192,2048]{2,1,0:T(8,128)(2,1)S(1)}, u32[]{:S(2)}, u32[]{:S(2)}) async-start(bf16[4,192,2048]{2,1,0:T(8,128)(2,1)} %bitcast.50), calls=%async_computation | async-start | bytes 6291456 | tf_op jit(solution)/shard_map/all_to_all | solution.py:27
  54.6 1.1 copy-start.4
  55.7 1.1 copy-start.5
  55.7 1.1 copy-start.7
  56.9 1.7 copy-start.8
  57.6 0.9 copy-start.2
  194.1 6.7 %copy-start.6 = (f32[192,2]{0,1:T(2,128)S(1)}, f32[192,2]{0,1:T(2,128)}, u32[]{:S(2)}) copy-start(f32[192,2]{0,1:T(2,128)} %param.26) | copy-start | bytes 4612
  194.1 6.8 %copy-start.11 = (f32[192]{0:T(256)S(1)}, f32[192]{0:T(256)}, u32[]{:S(2)}) copy-start(f32[192]{0:T(256)} %param.25) | copy-start | bytes 2308
  194.1 101.2 %all-to-all-start.3 = ((bf16[64,12,2048]{2,1,0:T(8,128)(2,1)}), bf16[64,12,2048]{2,1,0:T(8,128)(2,1)}, u32[]{:S(2)}, u32[]{:S(2)}) async-start(bf16[64,12,2048]{2,1,0:T(8,128)(2,1)} %reshape.174), calls=%async_computation.3 | async-start | bytes 8388608 | tf_op jit(solution)/shard_map/all_to_all | solution.py:122
  305.9 2.3 copy-start.3
  308.2 2.6 copy-start.1
where the time goes:
time: 312 us; the launch traced here: 311 us
  waiting for transfers between devices  129 us (41%)
  blocking collectives  90.5 us (29%)
  local copies, waits for them, and re-layouts  47.3 us (15%)
  starting transfers between devices  17.2 us (6%)
  matrix products  16.1 us (5%)
  other arithmetic  10.5 us (3%)
    all_to_all x1, waiting for transfers between devices, per_device(): lax.all_to_all(served, SP, split_axis=0, concat_axis=0, tiled=True)  94.3 us
    all_to_all x2, blocking collectives, turned_blocks(): out = lax.all_to_all(out, axes[k], k, k, tiled=True)  90.5 us
    all_to_all x1, waiting for transfers between devices, sent_and_summed(): parts = lax.all_to_all(split_up(value, dim, peers), axis, 0, 0, tiled=True)  34.6 us
    gather x2, local copies, waits for them, and re-layouts, per_device(): normed[source_of // per_token]  10.3 us
    dot_general x1, matrix products, per_device(): jnp.dot(inner_hidden, down_experts[0], preferred_element_type=jnp.float32)  7.9 us
    reshape x2, local copies, waits for them, and re-layouts, per_device(): returned.reshape(experts_all * capacity, -1)[slot_of]  7.49 us
    ppermute x2, starting transfers between devices, passed_along(): lax.ppermute(value, axis, [(source, source + steps) for source in range(l...  6.61 us
    all_to_all x1, starting transfers between devices, per_device(): lax.all_to_all(served, SP, split_axis=0, concat_axis=0, tiled=True)  6.45 us
  transfers between devices with their start and end apart: 4, of which 2 were waited for; matrix products, arithmetic and copies ran while one was open for 2% of the time, Pallas kernels for 0%

commit v1 on v0

v1 whole, which is shorter than its diff:
```python
import functools

import jax
import jax.numpy as jnp
from jax import lax
from jax.experimental import pallas as pl
from jax.experimental.pallas import tpu as pltpu
from jax.sharding import Mesh
from jax.sharding import PartitionSpec as P

Z, Y, CORE, X = "sp_0", "sp_1", "sp_2", "tp"
SP = (Z, Y, CORE)
SP_TP = (Z, Y, CORE, X)
MESH = pl.DeviceIdType.MESH

epsilon = 1e-06
WIDTH = 256


def passed_along(value, axis, steps):
    count = lax.axis_size(axis)
    leading, last = (max(0, -steps), min(count, count - steps))
    return lax.ppermute(value, axis, [(source, source + steps) for source in range(leading, last)])


def split_up(value, dim, peers):
    before, after = (value.shape[:dim], value.shape[dim + 1 :])
    return jnp.moveaxis(value.reshape(*before, peers, -1, *after), dim, 0)


def sent_and_summed(value, axis, dim):
    peers = lax.axis_size(axis)
    parts = lax.all_to_all(split_up(value, dim, peers), axis, 0, 0, tiled=True)
    return jnp.sum(parts.astype(jnp.float32), axis=0)


def rms_scale(values, gain):
    return values * lax.rsqrt(jnp.mean(values * values, axis=-1, keepdims=True) + epsilon) * gain


def dot32(a, b):
    return jnp.dot(a, b, preferred_element_type=jnp.float32)


def expert_kernel(
    zs, ys, cs, cap, slots,
    normed_ref, hidden_ref, pick_ref, meta_ref, whi_ref, wlo_ref, gate_hbm, up_hbm, down_hbm,
    out_ref,
    s1, r1, s2, r2, o2, b2, o1, b1, metar, onehot_t, onehot, acc, act, gate_v, up_v, down_v,
    z_send, z_recv, g_send, g_recv, bg_send, bg_recv, bz_send, bz_recv, m_send, m_recv, w_sem,
):
    z, y, c = lax.axis_index(Z), lax.axis_index(Y), lax.axis_index(CORE)
    groups = ys * cs
    g_me = y * cs + c
    chunks = s1.shape[0]
    width = s1.shape[3]
    bf = jnp.bfloat16

    weights = [
        pltpu.make_async_copy(src, dst, w_sem.at[i])
        for i, (src, dst) in enumerate(((gate_hbm, gate_v), (up_hbm, up_v), (down_hbm, down_v)))
    ]
    for copy in weights:
        copy.start()

    def z_peer(o):
        return lax.rem(z + o, zs)

    def g_peer(o):
        return lax.rem(g_me + o, groups)

    def g_device(g):
        return {Y: lax.div(g, cs), CORE: lax.rem(g, cs)}

    barrier = pltpu.get_barrier_semaphore()
    for o in range(1, zs):
        pl.semaphore_signal(barrier, inc=1, device_id={Z: z_peer(o)}, device_id_type=MESH)
    for o in range(1, groups):
        pl.semaphore_signal(barrier, inc=1, device_id=g_device(g_peer(o)), device_id_type=MESH)
    pl.semaphore_wait(barrier, zs + groups - 2)

    def z_copy(src, dst, send, recv, k, o):
        return pltpu.make_async_remote_copy(
            src_ref=src.at[k, z_peer(o)], dst_ref=dst.at[k, z],
            send_sem=send.at[k, o - 1], recv_sem=recv.at[k, o - 1],
            device_id={Z: z_peer(o)}, device_id_type=MESH,
        )

    def g_copy(src, dst, send, recv, k, o):
        return pltpu.make_async_remote_copy(
            src_ref=src.at[k, g_peer(o)], dst_ref=dst.at[k, g_me],
            send_sem=send.at[k, o - 1], recv_sem=recv.at[k, o - 1],
            device_id=g_device(g_peer(o)), device_id_type=MESH,
        )

    def m_copy(o):
        return pltpu.make_async_remote_copy(
            src_ref=meta_ref.at[z_peer(o)], dst_ref=metar.at[z],
            send_sem=m_send.at[o - 1], recv_sem=m_recv.at[o - 1],
            device_id={Z: z_peer(o)}, device_id_type=MESH,
        )

    z_sends = functools.partial(z_copy, s1, r1, z_send, z_recv)
    g_sends = functools.partial(g_copy, s2, r2, g_send, g_recv)
    g_backs = functools.partial(g_copy, o2, b2, bg_send, bg_recv)
    z_backs = functools.partial(z_copy, o1, b1, bz_send, bz_recv)

    def start_all(copies, k, count):
        for o in range(1, count):
            copies(k, o).start()

    def wait_recv_all(copies, k, count):
        for o in range(1, count):
            copies(k, o).wait_recv()

    for o in range(1, zs):
        m_copy(o).start()

    def columns(k):
        return pl.ds(pl.multiple_of(k * width, width), width)

    @pl.loop(0, chunks)
    def _(k):
        values = normed_ref[:, columns(k)]
        for j in range(zs):
            s1[k, j] = dot32(pick_ref[j * cap : (j + 1) * cap, :], values).astype(bf)
        start_all(z_sends, k, zs)
        r1[k, z] = s1[k, z]

    metar[z] = meta_ref[z]
    for o in range(1, zs):
        m_copy(o).wait_recv()
    total = groups * slots
    places = lax.broadcasted_iota(jnp.int32, (cap, total), 1).astype(jnp.float32)

    @pl.loop(0, zs)
    def _(j):
        where = jnp.transpose(metar[j])[:cap, 0:1]
        onehot_t[pl.ds(pl.multiple_of(j * cap, 16), cap), :] = jnp.where(
            where == places, jnp.ones((), jnp.float32), jnp.zeros((), jnp.float32)
        ).astype(bf)

    @pl.loop(0, zs * cap // 128)
    def _(j):
        rows = pl.ds(pl.multiple_of(j * 128, 128), 128)
        onehot[:, rows] = jnp.transpose(onehot_t[rows, :].astype(jnp.float32)).astype(bf)

    weights[0].wait()
    weights[1].wait()
    acc[...] = jnp.zeros_like(acc)
    hidden_units = gate_v.shape[1]

    @pl.loop(0, chunks + 1)
    def _(k):
        @pl.when(k < chunks)
        def _():
            wait_recv_all(z_sends, k, zs)
            rows = r1[k].reshape(zs * cap, width)
            for g in range(groups):
                s2[k, g] = dot32(onehot[g * slots : (g + 1) * slots, :], rows).astype(bf)
            start_all(g_sends, k, groups)
            r2[k, g_me] = s2[k, g_me]

        @pl.when(k >= 1)
        def _():
            b = k - 1
            wait_recv_all(g_sends, b, groups)
            ks = pl.ds(pl.multiple_of(b * width, width), width)
            for half in range(2):
                rows = r2[b, half * groups // 2 : (half + 1) * groups // 2].reshape(total // 2, width)
                at = slice(half * total // 2, (half + 1) * total // 2)
                acc[at, :hidden_units] += dot32(rows, gate_v[ks, :])
                acc[at, hidden_units:] += dot32(rows, up_v[ks, :])

    @pl.loop(0, groups)
    def _(g):
        at = pl.ds(pl.multiple_of(g * slots, slots), slots)
        first = acc[at, :hidden_units]
        second = acc[at, hidden_units:]
        act[at, :] = (first / (1.0 + jnp.exp(-first)) * second).astype(bf)

    weights[2].wait()

    @pl.loop(0, chunks)
    def _(k):
        down = down_v[:, columns(k)]
        for g in range(groups):
            o2[k, g] = dot32(act[g * slots : (g + 1) * slots, :], down).astype(bf)
        start_all(g_backs, k, groups)
        b2[k, g_me] = o2[k, g_me]

    @pl.loop(0, chunks)
    def _(k):
        wait_recv_all(g_backs, k, groups)
        rows = b2[k].reshape(total, width)
        for j in range(zs):
            o1[k, j] = dot32(onehot_t[j * cap : (j + 1) * cap, :], rows).astype(bf)
        start_all(z_backs, k, zs)
        b1[k, z] = o1[k, z]

    @pl.loop(0, chunks)
    def _(k):
        wait_recv_all(z_backs, k, zs)
        rows = b1[k].reshape(zs * cap, width)
        value = hidden_ref[:, columns(k)].astype(jnp.float32)
        value = value + (dot32(whi_ref[...], rows) + dot32(wlo_ref[...], rows))
        out_ref[:, columns(k)] = value.astype(bf)

    for o in range(1, zs):
        m_copy(o).wait_send()

    @pl.loop(0, chunks)
    def _(k):
        for o in range(1, zs):
            z_sends(k, o).wait_send()
            z_backs(k, o).wait_send()
        for o in range(1, groups):
            g_sends(k, o).wait_send()
            g_backs(k, o).wait_send()


def routed_experts(normed, hidden, expert_ids, weights, gate, up, down, cap):
    zs, ys, cs = lax.axis_size(Z), lax.axis_size(Y), lax.axis_size(CORE)
    groups = ys * cs
    tokens, model = normed.shape
    per_token = expert_ids.shape[1]
    experts = zs * groups
    limit = 2 * per_token * tokens // experts
    slots = zs * limit
    entries = tokens * per_token
    expert_of = expert_ids.reshape(-1)
    z_of = expert_of // groups
    order = jnp.arange(entries, dtype=jnp.int32)
    before = (order[None, :] < order[:, None]).astype(jnp.bfloat16)

    def rank(labels, count):
        onehot = labels[:, None] == jnp.arange(count, dtype=jnp.int32)[None, :]
        seen = dot32(before, onehot.astype(jnp.bfloat16))
        return jnp.sum(jnp.where(onehot, seen, 0.0), axis=1).astype(jnp.int32)

    slot_of = (expert_of % groups) * slots + lax.axis_index(Z) * limit + rank(expert_of, experts)
    row_of = z_of * cap + rank(z_of, zs)
    rows = zs * cap
    matched = row_of[None, :] == jnp.arange(rows, dtype=jnp.int32)[:, None]
    meta = jnp.sum(jnp.where(matched, (slot_of + 1)[None, :], 0), axis=1) - 1
    meta = jnp.pad(meta.reshape(zs, 1, cap), ((0, 0), (0, 7), (0, 128 - cap)), constant_values=-1)
    meta = meta.astype(jnp.float32)
    row_pair = row_of.reshape(tokens, per_token)
    row_ids = jnp.arange(rows, dtype=jnp.int32)
    pick = jnp.zeros((rows, tokens), bool)
    weigh = jnp.zeros((tokens, rows), jnp.float32)
    for k in range(per_token):
        pick = pick | (row_ids[:, None] == row_pair[None, :, k])
        weigh = weigh + jnp.where(row_ids[None, :] == row_pair[:, k : k + 1], weights[:, k : k + 1], 0.0)
    pick = pick.astype(jnp.bfloat16)
    whi = weigh.astype(jnp.bfloat16)
    wlo = (weigh - whi.astype(jnp.float32)).astype(jnp.bfloat16)
    chunks = model // WIDTH
    units = gate.shape[1]
    bf = jnp.bfloat16
    vmem, anywhere = pl.BlockSpec(memory_space=pltpu.VMEM), pl.BlockSpec(memory_space=pl.ANY)
    z_block, g_block = (chunks, zs, cap, WIDTH), (chunks, groups, slots, WIDTH)
    z_sem, g_sem = pltpu.SemaphoreType.DMA((chunks, zs - 1)), pltpu.SemaphoreType.DMA((chunks, groups - 1))
    m_sem = pltpu.SemaphoreType.DMA((zs - 1,))
    total = groups * slots
    return pl.pallas_call(
        functools.partial(expert_kernel, zs, ys, cs, cap, slots),
        out_shape=jax.ShapeDtypeStruct((tokens, model), bf),
        in_specs=[vmem] * 6 + [anywhere] * 3,
        out_specs=vmem,
        scratch_shapes=[
            pltpu.VMEM(z_block, bf), pltpu.VMEM(z_block, bf),
            pltpu.VMEM(g_block, bf), pltpu.VMEM(g_block, bf),
            pltpu.VMEM(g_block, bf), pltpu.VMEM(g_block, bf),
            pltpu.VMEM(z_block, bf), pltpu.VMEM(z_block, bf),
            pltpu.VMEM((zs, 8, 128), jnp.float32),
            pltpu.VMEM((rows, total), bf),
            pltpu.VMEM((total, rows), bf),
            pltpu.VMEM((total, 2 * units), jnp.float32),
            pltpu.VMEM((total, units), bf),
            pltpu.VMEM(gate.shape, bf), pltpu.VMEM(up.shape, bf), pltpu.VMEM(down.shape, bf),
            z_sem, z_sem, g_sem, g_sem, g_sem, g_sem, z_sem, z_sem, m_sem, m_sem,
            pltpu.SemaphoreType.DMA((3,)),
        ],
        compiler_params=pltpu.CompilerParams(
            collective_id=1, has_side_effects=True, vmem_limit_bytes=60 * 1024 * 1024
        ),
        name="routed_experts",
    )(normed, hidden, pick, meta, whi, wlo, gate, up, down)


def per_device(
    conv_outer,
    conv_inner,
    conv_input,
    conv_taps,
    out_weight,
    mix_gate,
    residual,
    mix_gain,
    expert_gain,
    expert_ids,
    group_share,
    pair_scores,
    gate_experts,
    up_experts,
    down_experts,
):
    kept = conv_taps.shape[0] - 1
    earlier = passed_along((conv_inner[-kept:], conv_input[-kept:]), SP, 1)
    inner = jnp.concatenate(
        [
            earlier[0].astype(jnp.float32) * earlier[1].astype(jnp.float32),
            conv_inner.astype(jnp.float32) * conv_input.astype(jnp.float32),
        ],
        0,
    )
    length = conv_inner.shape[0]
    conv = conv_taps[0] * inner[0:length]
    for offset in range(1, kept + 1):
        conv = conv + conv_taps[offset] * inner[offset : offset + length]
    mixed_rows = (conv_outer.astype(jnp.float32) * conv).astype(jnp.bfloat16)
    projected = sent_and_summed(
        jnp.dot(mixed_rows, out_weight, preferred_element_type=jnp.float32).astype(jnp.bfloat16),
        X,
        0,
    )
    mixed = jax.nn.sigmoid(mix_gate.astype(jnp.float32)) * projected
    hidden_state = (residual.astype(jnp.float32) + rms_scale(mixed, mix_gain)).astype(jnp.bfloat16)
    normed = rms_scale(hidden_state.astype(jnp.float32), expert_gain).astype(jnp.bfloat16)
    weights = group_share[:, None] * jax.nn.softmax(pair_scores, axis=-1)
    limit = 2 * expert_ids.shape[1] * residual.shape[0] // (lax.axis_size(SP) * gate_experts.shape[0])
    cap = limit * lax.axis_size(Y) * lax.axis_size(CORE)
    return routed_experts(
        normed, hidden_state, expert_ids, weights, gate_experts[0], up_experts[0], down_experts[0], cap
    )


def solution(mesh):
    torus = Mesh(mesh.devices.reshape(8, 4, 2, mesh.shape["tp"]), SP_TP)
    return jax.shard_map(
        per_device,
        mesh=torus,
        in_specs=(
            P(SP, X),
            P(SP, X),
            P(SP, X),
            P(None, X),
            P(X, None),
            P(SP_TP, None),
            P(SP_TP, None),
            P(),
            P(),
            P(SP_TP, None),
            P(SP_TP),
            P(SP_TP, None),
            P(SP, None, None),
            P(SP, None, None),
            P(SP, None, None),
        ),
        out_specs=P(SP_TP, None),
        check_vma=False,
    )
```

time: 312 us -> 240 us (0.77)
  Pallas kernels: 0 us -> 172 us
  waiting for transfers between devices: 129 us -> 33.4 us
  blocking collectives: 90.5 us -> 0 us
  local copies, waits for them, and re-layouts: 47.3 us -> 5.11 us
  matrix products: 16.1 us -> 6.73 us
  starting transfers between devices: 17.2 us -> 11.4 us
    pallas_call x0 -> x1, Pallas kernels: none -> 172 us  [routed_experts(): pl.pallas_call(functools.partial(expert_kernel, zs, ys, cs, cap, slots),...]
    all_to_all x1 -> x0, waiting for transfers between devices: 94.3 us -> none  [per_device(): lax.all_to_all(served, SP, split_axis=0, concat_axis=0, tiled=True)]
    all_to_all x2 -> x0, blocking collectives: 90.5 us -> none  [turned_blocks(): out = lax.all_to_all(out, axes[k], k, k, tiled=True)]
    reshape x4 -> x1, local copies, waits for them, and re-layouts: 13.7 us -> 0.14 us  [routed_experts(): expert_of = expert_ids.reshape(-1)]
    gather x3 -> x0, local copies, waits for them, and re-layouts: 13.5 us -> none  [the longest x2 10.3 us: per_device(): normed[source_of // per_token]]
    dot_general x2, matrix products: 12.4 us -> 0.42 us  [dot32(): return jnp.dot(a, b, preferred_element_type=jnp.float32)]
    all_to_all x1 -> x0, starting transfers between devices: 6.45 us -> none  [per_device(): lax.all_to_all(served, SP, split_axis=0, concat_axis=0, tiled=True)]
    all_to_all x2 -> x0, local copies, waits for them, and re-layouts: 5.42 us -> none  [turned_blocks(): out = lax.all_to_all(out, axes[k], k, k, tiled=True)]
  transfers between devices with their start and end apart: 4 -> 3, of which waited for: 2 -> 1; matrix products, arithmetic and copies ran while one was open for 2% -> 3% of each run, Pallas kernels for 0% -> 0%
where the time goes in v1:
time: 240 us; the launch traced here: 239 us
  Pallas kernels  172 us (72%)
  waiting for transfers between devices  33.4 us (14%)
  starting transfers between devices  11.4 us (5%)
  other arithmetic  10.8 us (4%)
  matrix products  6.73 us (3%)
  local copies, waits for them, and re-layouts  5.11 us (2%)
    pallas_call x1, Pallas kernels, routed_experts(): pl.pallas_call(functools.partial(expert_kernel, zs, ys, cs, cap, slots),...  172 us
    all_to_all x1, waiting for transfers between devices, sent_and_summed(): parts = lax.all_to_all(split_up(value, dim, peers), axis, 0, 0, tiled=True)  33.4 us
    ppermute x2, starting transfers between devices, passed_along(): lax.ppermute(value, axis, [(source, source + steps) for source in range(l...  6.62 us
    dot_general x1, matrix products, per_device(): jnp.dot(mixed_rows, out_weight, preferred_element_type=jnp.float32)  6.31 us
  transfers between devices with their start and end apart: 3, of which 1 were waited for; matrix products, arithmetic and copies ran while one was open for 3% of the time, Pallas kernels for 0%

profile of v1, /device:TPU:1, one launch (start us, length us, event | category | flops | bytes accessed | tf_op | source)
XLA Modules:
  0.0 239.3 jit_solution(6621707131218436430)
XLA Ops:
  0.0 0.0 copy-start
  0.0 0.9 slice.36
  0.9 4.6 %collective-permute-start = (bf16[2,512]{1,0:T(2,128)(2,1)S(1)}, bf16[2,512]{1,0:T(2,128)(2,1)S(1)}, u32[]{:S(2)}, u32[]{:S(2)}) collective-permute-start(bf16[2,512]{1,0:T(2,128)(2,1)S(1)} %slice.36), channel_id=1, source_target_pairs={{0,4},{4,8},{8,12},{12,16},{16,20},{20,24},{24,28},{28,32},{32,36}... | collective-permute-start | bytes 6152 | tf_op jit(solution)/shard_map/ppermute | solution.py:23
  5.4 0.7 slice.37
  6.1 0.0 copy-start.8
  6.1 0.0 copy-start.7
  6.1 0.0 copy-start.10
  6.1 2.1 collective-permute-start.1
  8.2 2.7 %convert_multiply_fusion.2 = f32[768,512]{1,0:T(8,128)} fusion(bf16[768,512]{1,0:T(8,128)(2,1)} %param.17, bf16[768,512]{1,0:T(8,128)(2,1)} %param.16), kind=kLoop, calls=%fused_computation.19 | loop fusion | flops 1179648 | bytes 3145728 | tf_op jit(solution)/shard_map/mul | solution.py:314
  11.0 0.0 copy-done.8
  11.0 0.0 copy-done.7
  11.0 0.1 copy.32
  11.1 0.1 reshape.136
  11.2 0.2 fusion.10
  11.5 0.0 collective-permute-done
  11.5 0.0 collective-permute-done.1
  11.5 0.0 copy-done
  11.5 0.0 copy-done.10
  11.6 6.3 %convolution_convert_fusion = bf16[768,2048]{1,0:T(8,128)(2,1)} fusion(bf16[512,2048]{1,0:T(8,128)(2,1)S(1)} %copy-done, f32[2,512]{1,0:T(2,128)S(1)} %convert_multiply_fusion.3, f32[768,512]{1,0:T(8,128)} %convert_multiply_fusion.2, bf16[768,512]{1,0:T(8,128)(2,1)S(1)} %copy-done.10, f32[512]{0:T(512)S(1)} %bitcast.17, f32[512]{0:T(512)S(1)} %bitcast.18, ...), kind=kOutput, calls=%fused_computation.1 | convolution fusion | flops 1616117760 | bytes 7612416 | tf_op jit(solution)/shard_map/dot_general | solution.py:324
  17.9 0.0 copy-start.4
  17.9 0.0 copy-start.9
  17.9 4.8 %all-to-all-start = ((bf16[4,192,2048]{2,1,0:T(8,128)(2,1)}), bf16[4,192,2048]{2,1,0:T(8,128)(2,1)}, u32[]{:S(2)}, u32[]{:S(2)}) async-start(bf16[4,192,2048]{2,1,0:T(8,128)(2,1)} %bitcast.10), calls=%async_computation | async-start | bytes 6291456 | tf_op jit(solution)/shard_map/all_to_all | solution.py:33
  22.6 0.2 fusion.11
  22.9 0.1 convert_element_type.89
  23.0 0.2 copy.37
  23.2 0.2 select_reduce_fusion
  23.4 0.1 sub.28
  23.5 0.0 copy-done.4
  23.5 0.6 pad_convert_fusion.meta_ref
  24.1 0.1 fusion.21
  24.2 0.2 slice_reduce_fusion.1
  24.4 0.0 copy-done.9
  24.4 0.9 fusion.17.pick_ref
  25.4 1.1 subtract_convert_fusion
  26.4 33.4 %all-to-all-done = bf16[4,192,2048]{2,1,0:T(8,128)(2,1)} async-done(((bf16[4,192,2048]{2,1,0:T(8,128)(2,1)}), bf16[4,192,2048]{2,1,0:T(8,128)(2,1)}, u32[]{:S(2)}, u32[]{:S(2)}) %all-to-all-start) | async-done | bytes 3145760 | tf_op jit(solution)/shard_map/all_to_all | solution.py:33
  59.9 2.7 %convert_reduce_fusion = f32[192,2048]{1,0:T(8,128)S(1)} fusion(bf16[4,192,2048]{2,1,0:T(8,128)(2,1)} %all-to-all-done), kind=kLoop, calls=%fused_computation | loop fusion | flops 2752512 | bytes 4718592 | tf_op jit(solution)/shard_map/reduce_sum | solution.py:34
  62.6 0.0 copy-done.2
  62.6 0.0 copy-start.3
  62.6 0.0 copy-start.5
  62.6 0.5 multiply_reduce_fusion
  63.1 0.6 copy-done.3
  63.7 0.0 copy-done.5
  63.7 0.8 fusion.6
  64.5 0.0 copy-done.6
  64.5 1.1 fusion.8.normed_ref
  65.6 0.0 copy-done.1
  65.6 171.5 %routed_experts.1 = bf16[192,2048]{1,0:T(8,128)(2,1)} custom-call(bf16[192,2048]{1,0:T(8,128)(2,1)} %fusion.8.normed_ref, bf16[192,2048]{1,0:T(8,128)(2,1)} %copy-done.1, bf16[768,192]{1,0:T(8,128)(2,1)} %fusion.17.pick_ref, f32[8,8,128]{2,1,0:T(8,128)} %pad_convert_fusion.meta_ref, bf16[192,768]{1,0:T(8,128)(2,1)} %get-tuple-element.13.whi_ref, ...), custom_call_target="tpu_custom_call" | custom-call | tf_op jit(solution)/shard_map/routed_experts/pallas_call | solution.py:266
  237.2 2.1 copy.42
  (16 shorter events, 0.1 us)
Async XLA Ops:
  0.0 11.5 %copy-start = (bf16[512,2048]{1,0:T(8,128)(2,1)S(1)}, bf16[512,2048]{1,0:T(8,128)(2,1)}, u32[]{:S(2)}) copy-start(bf16[512,2048]{1,0:T(8,128)(2,1)} %param.19) | copy-start | bytes 6291460
  0.9 10.6 %collective-permute-start = (bf16[2,512]{1,0:T(2,128)(2,1)S(1)}, bf16[2,512]{1,0:T(2,128)(2,1)S(1)}, u32[]{:S(2)}, u32[]{:S(2)}) collective-permute-start(bf16[2,512]{1,0:T(2,128)(2,1)S(1)} %slice.36), channel_id=1, source_target_pairs={{0,4},{4,8},{8,12},{12,16},{16,20},{20,24},{24,28},{28,32},{32,36}... | collective-permute-start | bytes 6152 | tf_op jit(solution)/shard_map/ppermute | solution.py:23
  6.1 4.8 %copy-start.8 = (f32[3,512]{1,0:T(4,128)S(1)}, f32[3,512]{1,0:T(4,128)}, u32[]{:S(2)}) copy-start(f32[3,512]{1,0:T(4,128)} %param.18) | copy-start | bytes 18436
  6.1 4.8 %copy-start.7 = (s32[192,2]{0,1:T(2,128)S(1)}, s32[192,2]{0,1:T(2,128)}, u32[]{:S(2)}) copy-start(s32[192,2]{0,1:T(2,128)} %param.24) | copy-start | bytes 4612
  6.1 5.4 %copy-start.10 = (bf16[768,512]{1,0:T(8,128)(2,1)S(1)}, bf16[768,512]{1,0:T(8,128)(2,1)}, u32[]{:S(2)}) copy-start(bf16[768,512]{1,0:T(8,128)(2,1)} %param.15) | copy-start | bytes 2359300
  6.1 5.4 %collective-permute-start.1 = (bf16[2,512]{1,0:T(2,128)(2,1)S(1)}, bf16[2,512]{1,0:T(2,128)(2,1)S(1)}, u32[]{:S(2)}, u32[]{:S(2)}) collective-permute-start(bf16[2,512]{1,0:T(2,128)(2,1)S(1)} %slice.37), channel_id=1, source_target_pairs={{0,4},{4,8},{8,12},{12,16},{16,20},{20,24},{24,28},{28,32},{32,36}... | collective-permute-start | bytes 6152 | tf_op jit(solution)/shard_map/ppermute | solution.py:23
  17.9 5.6 %copy-start.4 = (f32[192,2]{0,1:T(2,128)S(1)}, f32[192,2]{0,1:T(2,128)}, u32[]{:S(2)}) copy-start(f32[192,2]{0,1:T(2,128)} %param.26) | copy-start | bytes 4612
  17.9 6.5 %copy-start.9 = (f32[192]{0:T(256)S(1)}, f32[192]{0:T(256)}, u32[]{:S(2)}) copy-start(f32[192]{0:T(256)} %param.25) | copy-start | bytes 2308
  17.9 42.0 %all-to-all-start = ((bf16[4,192,2048]{2,1,0:T(8,128)(2,1)}), bf16[4,192,2048]{2,1,0:T(8,128)(2,1)}, u32[]{:S(2)}, u32[]{:S(2)}) async-start(bf16[4,192,2048]{2,1,0:T(8,128)(2,1)} %bitcast.10), calls=%async_computation | async-start | bytes 6291456 | tf_op jit(solution)/shard_map/all_to_all | solution.py:33
  26.4 36.1 %copy-start.2 = (bf16[192,2048]{1,0:T(8,128)(2,1)S(1)}, bf16[192,2048]{1,0:T(8,128)(2,1)}, u32[]{:S(2)}) copy-start(bf16[192,2048]{1,0:T(8,128)(2,1)} %param.20) | copy-start | bytes 2359300
  62.6 1.1 copy-start.3
  62.6 1.1 copy-start.5
  63.7 0.8 copy-start.6
  64.5 1.2 copy-start.1

commit v2 on v1

--- a/solution.py
+++ b/solution.py
@@ -15,23 +15,7 @@
 
 epsilon = 1e-06
 WIDTH = 256
-
-
-def passed_along(value, axis, steps):
-    count = lax.axis_size(axis)
-    leading, last = (max(0, -steps), min(count, count - steps))
-    return lax.ppermute(value, axis, [(source, source + steps) for source in range(leading, last)])
-
-
-def split_up(value, dim, peers):
-    before, after = (value.shape[:dim], value.shape[dim + 1 :])
-    return jnp.moveaxis(value.reshape(*before, peers, -1, *after), dim, 0)
-
-
-def sent_and_summed(value, axis, dim):
-    peers = lax.axis_size(axis)
-    parts = lax.all_to_all(split_up(value, dim, peers), axis, 0, 0, tiled=True)
-    return jnp.sum(parts.astype(jnp.float32), axis=0)
+USUAL = 80
 
 
 def rms_scale(values, gain):
@@ -42,11 +26,282 @@
     return jnp.dot(a, b, preferred_element_type=jnp.float32)
 
 
+def mixer_kernel(
+    sizes, limit, parts,
+    taps_ref, mix_gain_ref, expert_gain_ref, ids_ref, share_ref, scores_ref,
+    outer_hbm, inner_hbm, input_hbm, weight_hbm, gate_hbm, residual_hbm,
+    hidden_ref, normed_ref, columns_ref, lanes_ref, most_ref,
+    outer_v, inner_v, input_v, weight_v, gate_v, residual_v,
+    products, mixed, own, far, far_in, near, near_in, tails, tail_in, table,
+    mine, x_in, g_in, z_in, sent_x, sent_g,
+    l_sem, t_send, t_recv, f_send, f_recv, n_send, n_recv, mx_send, mx_recv, mg_send, mg_recv, mz_send, mz_recv,
+):
+    zs, ys, cs, xs = sizes
+    z, y, c, x = (lax.axis_index(a) for a in SP_TP)
+    groups = ys * cs
+    g_me = y * cs + c
+    devices = zs * groups
+    me = z * groups + g_me
+    bf, f32 = jnp.bfloat16, jnp.float32
+    length, lanes = inner_v.shape
+    rows = length // xs
+    half = own.shape[1] // 2
+    piece = rows // parts
+
+    loads = [
+        pltpu.make_async_copy(src, dst, l_sem.at[i])
+        for i, (src, dst) in enumerate(
+            (
+                (inner_hbm, inner_v), (input_hbm, input_v), (outer_hbm, outer_v),
+                (weight_hbm, weight_v), (gate_hbm, gate_v), (residual_hbm, residual_v),
+            )
+        )
+    ]
+    for load in loads:
+        load.start()
+
+    def sp_device(index):
+        return {Z: lax.div(index, groups), Y: lax.div(lax.rem(index, groups), cs), CORE: lax.rem(index, cs)}
+
+    following, preceding = lax.rem(me + 1, devices), lax.rem(me + devices - 1, devices)
+    x_peers = [{X: lax.rem(x + o, xs)} for o in range(1, xs)]
+    z_peers = [{Z: lax.rem(z + o, zs)} for o in range(1, zs)]
+    g_peers = []
+    for o in range(1, groups):
+        g = lax.rem(g_me + o, groups)
+        g_peers.append({Y: lax.div(g, cs), CORE: lax.rem(g, cs)})
+    everyone = x_peers + z_peers + g_peers + [sp_device(following), sp_device(preceding)]
+    barrier = pltpu.get_barrier_semaphore()
+    for peer in everyone:
+        pl.semaphore_signal(barrier, inc=1, device_id=peer, device_id_type=MESH)
+
+    loads[0].wait()
+    loads[1].wait()
+    last = tails.shape[1]
+    tails[0] = inner_v[length - last :, :]
+    tails[1] = input_v[length - last :, :]
+    pl.semaphore_wait(barrier, len(everyone))
+    tail_copy = pltpu.make_async_remote_copy(
+        src_ref=tails, dst_ref=tail_in, send_sem=t_send, recv_sem=t_recv,
+        device_id=sp_device(following), device_id_type=MESH,
+    )
+    tail_copy.start()
+
+    pad = 8
+    for b in range(xs):
+        at = slice(b * rows, (b + 1) * rows)
+        products[pad + b * rows : pad + (b + 1) * rows, :] = inner_v[at, :].astype(f32) * input_v[at, :].astype(f32)
+    loads[2].wait()
+    for b in reversed(range(xs)):
+        if b == 0:
+            tail_copy.wait_recv()
+            earlier = tail_in[0].astype(f32) * tail_in[1].astype(f32)
+            earlier = jnp.where(me == 0, jnp.zeros_like(earlier), earlier)
+            products[0:pad, :] = earlier[last - pad :, :]
+        start = b * rows
+        conv = taps_ref[0:1, :] * products[start + pad - 2 : start + pad - 2 + rows, :]
+        conv = conv + taps_ref[1:2, :] * products[start + pad - 1 : start + pad - 1 + rows, :]
+        conv = conv + taps_ref[2:3, :] * products[start + pad : start + pad + rows, :]
+        mixed[start : start + rows, :] = (outer_v[start : start + rows, :].astype(f32) * conv).astype(bf)
+    loads[3].wait()
+
+    right, left = lax.rem(x + 1, xs), lax.rem(x + xs - 1, xs)
+    ways = (right, left)
+
+    def partial_of(owner, h):
+        block = mixed[pl.ds(pl.multiple_of(owner * rows, 16), rows), :]
+        return dot32(block, weight_v[:, h * half : (h + 1) * half])
+
+    def far_copy(h, t):
+        at = pl.ds(t * piece, piece)
+        return pltpu.make_async_remote_copy(
+            src_ref=far.at[h, at], dst_ref=far_in.at[h, at],
+            send_sem=f_send.at[h, t], recv_sem=f_recv.at[h, t],
+            device_id={X: ways[h]}, device_id_type=MESH,
+        )
+
+    def near_copy(d, h, t):
+        at = pl.ds(t * piece, piece)
+        return pltpu.make_async_remote_copy(
+            src_ref=near.at[d, h, at], dst_ref=near_in.at[d, h, at],
+            send_sem=n_send.at[d, h, t], recv_sem=n_recv.at[d, h, t],
+            device_id={X: ways[d]}, device_id_type=MESH,
+        )
+
+    opposite = lax.rem(x + 2, xs)
+    for h in range(2):
+        far[h] = partial_of(opposite, h).astype(bf)
+        for t in range(parts):
+            far_copy(h, t).start()
+    for d in range(2):
+        near[d, 1 - d] = partial_of(ways[d], 1 - d).astype(bf)
+        for t in range(parts):
+            near_copy(d, 1 - d, t).start()
+    for d in range(2):
+        own[:, d * half : (d + 1) * half] = partial_of(ways[d], d)
+
+    tokens = ids_ref.shape[0]
+    expert = [ids_ref[:, k : k + 1].astype(f32) for k in range(2)]
+    z_of = [jnp.floor((e + 0.5) / groups) for e in expert]
+    lane = lax.broadcasted_iota(jnp.int32, (tokens, 128), 1).astype(f32)
+    marks = [
+        jnp.where((e == lane) | (zz + devices == lane), jnp.ones((), f32), jnp.zeros((), f32))
+        for e, zz in zip(expert, z_of)
+    ]
+    before = jnp.where(
+        lax.broadcasted_iota(jnp.int32, (tokens, tokens), 1) < lax.broadcasted_iota(jnp.int32, (tokens, tokens), 0),
+        jnp.ones((), f32), jnp.zeros((), f32),
+    ).astype(bf)
+    first_sum = jnp.sum(marks[0], axis=0, keepdims=True)
+    most = first_sum + jnp.sum(marks[1], axis=0, keepdims=True)
+    most = jnp.where(lane[0:1, :] >= devices, most, jnp.zeros_like(most))
+    most = jnp.broadcast_to(jnp.max(most, axis=1, keepdims=True), (8, 128))
+    mine[...] = most
+
+    def flag_copy(src, dst, send, recv, i, peer):
+        return pltpu.make_async_remote_copy(
+            src_ref=src, dst_ref=dst.at[i], send_sem=send.at[i], recv_sem=recv.at[i],
+            device_id=peer, device_id_type=MESH,
+        )
+
+    x_flags = [flag_copy(mine, x_in, mx_send, mx_recv, i, p) for i, p in enumerate(x_peers)]
+    g_flags = [flag_copy(sent_x, g_in, mg_send, mg_recv, i, p) for i, p in enumerate(g_peers)]
+    z_flags = [flag_copy(sent_g, z_in, mz_send, mz_recv, i, p) for i, p in enumerate(z_peers)]
+    for flag in x_flags:
+        flag.start()
+
+    seen = [dot32(before, marks[0].astype(bf)), dot32(before, marks[1].astype(bf)) + first_sum]
+    info = []
+    scores = [scores_ref[:, k : k + 1] for k in range(2)]
+    top = jnp.maximum(scores[0], scores[1])
+    powers = [jnp.exp(v - top) for v in scores]
+    for k in range(2):
+        hit = marks[k] * seen[k]
+        rank = jnp.sum(jnp.where(lane < devices, hit, 0.0), axis=1, keepdims=True)
+        place = jnp.sum(jnp.where(lane >= devices, hit, 0.0), axis=1, keepdims=True)
+        slot = (expert[k] - groups * z_of[k]) * (zs * limit) + (z * limit).astype(f32) + rank
+        info.append((z_of[k], place, slot, share_ref[...] * (powers[k] / (powers[0] + powers[1]))))
+    column = jnp.zeros((tokens, 128), f32)
+    for i in range(4):
+        for k in range(2):
+            column = column + jnp.where(lane == 2 * i + k, info[k][i], 0.0)
+    columns_ref[...] = column
+    table[...] = jnp.zeros_like(table)
+    table[0:tokens, :] = column
+    lanes_ref[...] = jnp.transpose(table[...])[0:8, :]
+
+    for flag in x_flags:
+        flag.wait_recv()
+    for i in range(xs - 1):
+        most = jnp.maximum(most, x_in[i])
+    sent_x[...] = most
+    for flag in g_flags:
+        flag.start()
+
+    for t in range(parts):
+        at = slice(t * piece, (t + 1) * piece)
+        for d in range(2):
+            far_copy(d, t).wait_recv()
+            near[d, d, at, :] = (own[at, d * half : (d + 1) * half] + far_in[d, at, :].astype(f32)).astype(bf)
+            near_copy(d, d, t).start()
+    for h in range(2):
+        own[:, h * half : (h + 1) * half] = partial_of(x, h)
+
+    for flag in g_flags:
+        flag.wait_recv()
+    for i in range(groups - 1):
+        most = jnp.maximum(most, g_in[i])
+    sent_g[...] = most
+    for flag in z_flags:
+        flag.start()
+
+    loads[4].wait()
+    loads[5].wait()
+    for t in range(parts):
+        at = slice(t * piece, (t + 1) * piece)
+        for d in range(2):
+            for h in range(2):
+                near_copy(d, h, t).wait_recv()
+        sums = []
+        for h in range(2):
+            part = own[at, h * half : (h + 1) * half]
+            sums.append(part + near_in[0, h, at, :].astype(f32) + near_in[1, h, at, :].astype(f32))
+        projected = jnp.concatenate(sums, axis=1)
+        value = jax.nn.sigmoid(gate_v[at, :].astype(f32)) * projected
+        hidden = (residual_v[at, :].astype(f32) + rms_scale(value, mix_gain_ref[...])).astype(bf)
+        hidden_ref[at, :] = hidden
+        normed_ref[at, :] = rms_scale(hidden.astype(f32), expert_gain_ref[...]).astype(bf)
+
+    for flag in z_flags:
+        flag.wait_recv()
+    for i in range(zs - 1):
+        most = jnp.maximum(most, z_in[i])
+    most_ref[...] = most
+
+    tail_copy.wait_send()
+    for h in range(2):
+        for t in range(parts):
+            far_copy(h, t).wait_send()
+            for d in range(2):
+                near_copy(d, h, t).wait_send()
+    for flag in x_flags + g_flags + z_flags:
+        flag.wait_send()
+
+
+def mixer(outer, inner, values, taps, weight, gate, residual, mix_gain, expert_gain, ids, share, scores, limit):
+    sizes = tuple(lax.axis_size(a) for a in SP_TP)
+    zs, ys, cs, xs = sizes
+    groups = ys * cs
+    length, lanes = inner.shape
+    rows, model = residual.shape
+    half, parts, last = model // 2, 4, 16
+    bf, f32 = jnp.bfloat16, jnp.float32
+    vmem, anywhere = pl.BlockSpec(memory_space=pltpu.VMEM), pl.BlockSpec(memory_space=pl.ANY)
+    dma = pltpu.SemaphoreType.DMA
+    flag = (8, 128)
+    return pl.pallas_call(
+        functools.partial(mixer_kernel, sizes, limit, parts),
+        out_shape=(
+            jax.ShapeDtypeStruct((rows, model), bf),
+            jax.ShapeDtypeStruct((rows, model), bf),
+            jax.ShapeDtypeStruct((rows, 128), f32),
+            jax.ShapeDtypeStruct((8, 256), f32),
+            jax.ShapeDtypeStruct(flag, f32),
+        ),
+        in_specs=[vmem] * 6 + [anywhere] * 6,
+        out_specs=(vmem,) * 5,
+        scratch_shapes=[
+            pltpu.VMEM(outer.shape, bf), pltpu.VMEM(inner.shape, bf), pltpu.VMEM(values.shape, bf),
+            pltpu.VMEM(weight.shape, bf), pltpu.VMEM(gate.shape, bf), pltpu.VMEM(residual.shape, bf),
+            pltpu.VMEM((length + 8, lanes), f32),
+            pltpu.VMEM((length, lanes), bf),
+            pltpu.VMEM((rows, model), f32),
+            pltpu.VMEM((2, rows, half), bf), pltpu.VMEM((2, rows, half), bf),
+            pltpu.VMEM((2, 2, rows, half), bf), pltpu.VMEM((2, 2, rows, half), bf),
+            pltpu.VMEM((2, last, lanes), bf), pltpu.VMEM((2, last, lanes), bf),
+            pltpu.VMEM((256, 128), f32),
+            pltpu.VMEM(flag, f32), pltpu.VMEM((xs - 1, *flag), f32),
+            pltpu.VMEM((groups - 1, *flag), f32), pltpu.VMEM((zs - 1, *flag), f32),
+            pltpu.VMEM(flag, f32), pltpu.VMEM(flag, f32),
+            dma((6,)), dma, dma,
+            dma((2, parts)), dma((2, parts)), dma((2, 2, parts)), dma((2, 2, parts)),
+            dma((xs - 1,)), dma((xs - 1,)), dma((groups - 1,)), dma((groups - 1,)), dma((zs - 1,)), dma((zs - 1,)),
+        ],
+        compiler_params=pltpu.CompilerParams(
+            collective_id=1, has_side_effects=True, vmem_limit_bytes=48 * 1024 * 1024
+        ),
+        name="mixer",
+    )(
+        taps, mix_gain[None, :], expert_gain[None, :], ids, share[:, None], scores,
+        outer, inner, values, weight, gate, residual,
+    )
+
+
 def expert_kernel(
     zs, ys, cs, cap, slots,
-    normed_ref, hidden_ref, pick_ref, meta_ref, whi_ref, wlo_ref, gate_hbm, up_hbm, down_hbm,
+    normed_ref, hidden_ref, columns_ref, lanes_ref, gate_hbm, up_hbm, down_hbm,
     out_ref,
-    s1, r1, s2, r2, o2, b2, o1, b1, metar, onehot_t, onehot, acc, act, gate_v, up_v, down_v,
+    pick_ref, meta_ref, whi_ref, wlo_ref, s1, r1, s2, r2, o2, b2, o1, b1, metar, onehot_t, onehot, acc, act, gate_v, up_v, down_v,
     z_send, z_recv, g_send, g_recv, bg_send, bg_recv, bz_send, bz_recv, m_send, m_recv, w_sem,
 ):
     z, y, c = lax.axis_index(Z), lax.axis_index(Y), lax.axis_index(CORE)
@@ -113,11 +368,17 @@
         for o in range(1, count):
             copies(k, o).wait_recv()
 
-    for o in range(1, zs):
-        m_copy(o).start()
-
     def columns(k):
         return pl.ds(pl.multiple_of(k * width, width), width)
+
+    f32 = jnp.float32
+    tokens = normed_ref.shape[0]
+    row_of = [lanes_ref[k : k + 1, 0:tokens] * cap + lanes_ref[2 + k : 3 + k, 0:tokens] for k in range(2)]
+    slot_of = [lanes_ref[4 + k : 5 + k, 0:tokens] + 1.0 for k in range(2)]
+    place = lax.broadcasted_iota(jnp.int32, (cap, tokens), 0).astype(f32)
+    for j in range(zs):
+        hit = [place + float(j * cap) == r for r in row_of]
+        pick_ref[j * cap : (j + 1) * cap, :] = jnp.where(hit[0] | hit[1], jnp.ones((), f32), jnp.zeros((), f32)).astype(bf)
 
     @pl.loop(0, chunks)
     def _(k):
@@ -127,6 +388,21 @@
         start_all(z_sends, k, zs)
         r1[k, z] = s1[k, z]
 
+    for j in range(zs):
+        hit = [place + float(j * cap) == r for r in row_of]
+        found = jnp.where(hit[0], slot_of[0], 0.0) + jnp.where(hit[1], slot_of[1], 0.0)
+        found = jnp.broadcast_to(jnp.sum(found, axis=1, keepdims=True) - 1.0, (cap, 128))
+        found = jnp.concatenate([found, jnp.full((128 - cap, 128), -1.0, f32)], axis=0)
+        meta_ref[j] = jnp.transpose(found)[0:8, :]
+    for o in range(1, zs):
+        m_copy(o).start()
+    row_lane = lax.broadcasted_iota(jnp.int32, (tokens, zs * cap), 1).astype(f32)
+    weigh = jnp.zeros((tokens, zs * cap), f32)
+    for k in range(2):
+        row = columns_ref[:, k : k + 1] * cap + columns_ref[:, 2 + k : 3 + k]
+        weigh = weigh + jnp.where(row == row_lane, columns_ref[:, 6 + k : 7 + k], 0.0)
+    whi_ref[...] = weigh.astype(bf)
+    wlo_ref[...] = (weigh - whi_ref[...].astype(f32)).astype(bf)
     metar[z] = meta_ref[z]
     for o in range(1, zs):
         m_copy(o).wait_recv()
@@ -219,42 +495,12 @@
             g_backs(k, o).wait_send()
 
 
-def routed_experts(normed, hidden, expert_ids, weights, gate, up, down, cap):
+def routed_experts(cap, limit, collective, normed, hidden, columns, lanes, gate, up, down):
     zs, ys, cs = lax.axis_size(Z), lax.axis_size(Y), lax.axis_size(CORE)
     groups = ys * cs
     tokens, model = normed.shape
-    per_token = expert_ids.shape[1]
-    experts = zs * groups
-    limit = 2 * per_token * tokens // experts
     slots = zs * limit
-    entries = tokens * per_token
-    expert_of = expert_ids.reshape(-1)
-    z_of = expert_of // groups
-    order = jnp.arange(entries, dtype=jnp.int32)
-    before = (order[None, :] < order[:, None]).astype(jnp.bfloat16)
-
-    def rank(labels, count):
-        onehot = labels[:, None] == jnp.arange(count, dtype=jnp.int32)[None, :]
-        seen = dot32(before, onehot.astype(jnp.bfloat16))
-        return jnp.sum(jnp.where(onehot, seen, 0.0), axis=1).astype(jnp.int32)
-
-    slot_of = (expert_of % groups) * slots + lax.axis_index(Z) * limit + rank(expert_of, experts)
-    row_of = z_of * cap + rank(z_of, zs)
     rows = zs * cap
-    matched = row_of[None, :] == jnp.arange(rows, dtype=jnp.int32)[:, None]
-    meta = jnp.sum(jnp.where(matched, (slot_of + 1)[None, :], 0), axis=1) - 1
-    meta = jnp.pad(meta.reshape(zs, 1, cap), ((0, 0), (0, 7), (0, 128 - cap)), constant_values=-1)
-    meta = meta.astype(jnp.float32)
-    row_pair = row_of.reshape(tokens, per_token)
-    row_ids = jnp.arange(rows, dtype=jnp.int32)
-    pick = jnp.zeros((rows, tokens), bool)
-    weigh = jnp.zeros((tokens, rows), jnp.float32)
-    for k in range(per_token):
-        pick = pick | (row_ids[:, None] == row_pair[None, :, k])
-        weigh = weigh + jnp.where(row_ids[None, :] == row_pair[:, k : k + 1], weights[:, k : k + 1], 0.0)
-    pick = pick.astype(jnp.bfloat16)
-    whi = weigh.astype(jnp.bfloat16)
-    wlo = (weigh - whi.astype(jnp.float32)).astype(jnp.bfloat16)
     chunks = model // WIDTH
     units = gate.shape[1]
     bf = jnp.bfloat16
@@ -266,9 +512,11 @@
     return pl.pallas_call(
         functools.partial(expert_kernel, zs, ys, cs, cap, slots),
         out_shape=jax.ShapeDtypeStruct((tokens, model), bf),
-        in_specs=[vmem] * 6 + [anywhere] * 3,
+        in_specs=[vmem] * 4 + [anywhere] * 3,
         out_specs=vmem,
         scratch_shapes=[
+            pltpu.VMEM((rows, tokens), bf), pltpu.VMEM((zs, 8, 128), jnp.float32),
+            pltpu.VMEM((tokens, rows), bf), pltpu.VMEM((tokens, rows), bf),
             pltpu.VMEM(z_block, bf), pltpu.VMEM(z_block, bf),
             pltpu.VMEM(g_block, bf), pltpu.VMEM(g_block, bf),
             pltpu.VMEM(g_block, bf), pltpu.VMEM(g_block, bf),
@@ -283,10 +531,10 @@
             pltpu.SemaphoreType.DMA((3,)),
         ],
         compiler_params=pltpu.CompilerParams(
-            collective_id=1, has_side_effects=True, vmem_limit_bytes=60 * 1024 * 1024
+            collective_id=collective, has_side_effects=True, vmem_limit_bytes=60 * 1024 * 1024
         ),
         name="routed_experts",
-    )(normed, hidden, pick, meta, whi, wlo, gate, up, down)
+    )(normed, hidden, columns, lanes, gate, up, down)
 
 
 def per_device(
@@ -306,33 +554,19 @@
     up_experts,
     down_experts,
 ):
-    kept = conv_taps.shape[0] - 1
-    earlier = passed_along((conv_inner[-kept:], conv_input[-kept:]), SP, 1)
-    inner = jnp.concatenate(
-        [
-            earlier[0].astype(jnp.float32) * earlier[1].astype(jnp.float32),
-            conv_inner.astype(jnp.float32) * conv_input.astype(jnp.float32),
-        ],
-        0,
+    limit = 2 * expert_ids.shape[1] * residual.shape[0] // (lax.axis_size(SP) * gate_experts.shape[0])
+    worst = limit * lax.axis_size(Y) * lax.axis_size(CORE)
+    hidden, normed, columns, lanes, most = mixer(
+        conv_outer, conv_inner, conv_input, conv_taps, out_weight, mix_gate, residual, mix_gain, expert_gain,
+        expert_ids, group_share, pair_scores, limit,
     )
-    length = conv_inner.shape[0]
-    conv = conv_taps[0] * inner[0:length]
-    for offset in range(1, kept + 1):
-        conv = conv + conv_taps[offset] * inner[offset : offset + length]
-    mixed_rows = (conv_outer.astype(jnp.float32) * conv).astype(jnp.bfloat16)
-    projected = sent_and_summed(
-        jnp.dot(mixed_rows, out_weight, preferred_element_type=jnp.float32).astype(jnp.bfloat16),
-        X,
-        0,
-    )
-    mixed = jax.nn.sigmoid(mix_gate.astype(jnp.float32)) * projected
-    hidden_state = (residual.astype(jnp.float32) + rms_scale(mixed, mix_gain)).astype(jnp.bfloat16)
-    normed = rms_scale(hidden_state.astype(jnp.float32), expert_gain).astype(jnp.bfloat16)
-    weights = group_share[:, None] * jax.nn.softmax(pair_scores, axis=-1)
-    limit = 2 * expert_ids.shape[1] * residual.shape[0] // (lax.axis_size(SP) * gate_experts.shape[0])
-    cap = limit * lax.axis_size(Y) * lax.axis_size(CORE)
-    return routed_experts(
-        normed, hidden_state, expert_ids, weights, gate_experts[0], up_experts[0], down_experts[0], cap
+    arguments = (normed, hidden, columns, lanes, gate_experts[0], up_experts[0], down_experts[0])
+    usual = USUAL
+    return lax.cond(
+        most[0, 0] <= usual,
+        functools.partial(routed_experts, usual, limit, 2),
+        functools.partial(routed_experts, worst, limit, 3),
+        *arguments,
     )
 
 

time: 240 us -> 233 us (0.971)
  Pallas kernels: 172 us -> 220 us
  waiting for transfers between devices: 33.4 us -> 0 us
  starting transfers between devices: 11.4 us -> 0 us
  other arithmetic: 10.8 us -> 0 us
  matrix products: 6.73 us -> 0 us
  local copies, waits for them, and re-layouts: 5.11 us -> 11.5 us
    pallas_call x0 -> x1, Pallas kernels: none -> 41.1 us  [mixer(): pl.pallas_call(functools.partial(mixer_kernel, sizes, limit, parts), out_...]
    all_to_all x1 -> x0, waiting for transfers between devices: 33.4 us -> none  [sent_and_summed(): parts = lax.all_to_all(split_up(value, dim, peers), axis, 0, 0, tiled=True)]
    pallas_call x1, Pallas kernels: 172 us -> 179 us  [routed_experts(): pl.pallas_call(functools.partial(expert_kernel, zs, ys, cs, cap, slots),...]
    unnamed x24 -> x21, local copies, waits for them, and re-layouts: 2.84 us -> 10.2 us
    dot_general x3 -> x0, matrix products: 6.73 us -> none  [the longest x1 6.31 us: per_device(): jnp.dot(mixed_rows, out_weight, preferred_element_type=jnp.float32)]
    ppermute x2 -> x0, starting transfers between devices: 6.62 us -> none  [passed_along(): lax.ppermute(value, axis, [(source, source + steps) for source in range(l...]
    all_to_all x1 -> x0, starting transfers between devices: 4.77 us -> none  [sent_and_summed(): parts = lax.all_to_all(split_up(value, dim, peers), axis, 0, 0, tiled=True)]
    reduce_sum x5 -> x0, other arithmetic: 4.2 us -> none  [the longest x1 2.69 us: sent_and_summed(): return jnp.sum(parts.astype(jnp.float32), axis=0)]
  transfers between devices with their start and end apart: 3 -> 0, of which waited for: 1 -> 0; matrix products, arithmetic and copies ran while one was open for 3% -> 0% of each run, Pallas kernels for 0% -> 0%
where the time goes in v2:
time: 233 us
  Pallas kernels  220 us (94%)
  local copies, waits for them, and re-layouts  11.5 us (5%)
    pallas_call x1, Pallas kernels, routed_experts(): pl.pallas_call(functools.partial(expert_kernel, zs, ys, cs, cap, slots),...  179 us
    pallas_call x1, Pallas kernels, mixer(): pl.pallas_call(functools.partial(mixer_kernel, sizes, limit, parts), out_...  41.1 us
    unnamed x21, local copies, waits for them, and re-layouts  10.2 us

profile of v2, /device:TPU:1, one launch (start us, length us, event | category | flops | bytes accessed | tf_op | source)
XLA Modules:
  0.0 232.7 jit_solution(14523238446577387798)
XLA Ops:
  0.0 0.8 copy.20.ids_ref
  0.8 0.8 copy.21.share_ref
  1.6 0.8 copy.22.scores_ref
  2.4 0.0 copy-start
  2.4 1.1 copy-done
  3.5 0.0 copy-start.1
  3.5 1.1 copy-done.1
  4.7 0.0 copy-start.2
  4.7 1.1 copy-done.2
  5.8 0.0 copy-start.3
  5.8 1.1 copy-done.3
  6.9 0.0 copy-start.4
  6.9 1.1 copy-done.4
  8.1 0.0 copy-start.5
  8.1 0.7 copy-done.5
  8.8 0.0 copy-start.6
  8.8 0.7 copy-done.6
  9.5 0.0 copy-start.7
  9.5 0.7 copy-done.7
  10.2 0.0 copy-start.8
  10.2 41.1 %mixer.1 = (bf16[192,2048]{1,0:T(8,128)(2,1)S(1)}, bf16[192,2048]{1,0:T(8,128)(2,1)}, f32[192,128]{1,0:T(8,128)S(1)}, f32[8,256]{1,0:T(8,128)S(1)}, f32[8,128]{1,0:T(8,128)S(1)}) custom-call(f32[3,512]{1,0:T(4,128)S(1)} %copy-done.5, f32[1,2048]{1,0:T(1,128)S(1)} %bitcast.7, f32[1,2048]{1,0:T(1,128)S(1)} %bitcast.8, s32[192,2]{1,0:T(8,128)S(1)} %copy.20.ids_ref, ...), custom_call_target="tpu_custom_call" | custom-call | tf_op jit(solution)/shard_map/mixer/pallas_call | solution.py:262
  51.3 0.5 slice.3
  52.4 0.0 copy-done.8
  52.4 179.3 %conditional.1 = (bf16[192,2048]{1,0:T(8,128)(2,1)S(1)}) conditional(s32[]{:T(128)} %bitcast.3, (bf16[192,2048]{1,0:T(8,128)(2,1)}, bf16[192,2048]{1,0:T(8,128)(2,1)S(1)}, f32[192,128]{1,0:T(8,128)S(1)}, f32[8,256]{1,0:T(8,128)S(1)}, bf16[2048,512]{1,0:T(8,128)(2,1)S(1)}, /*index=5*/bf16[2048,512]{1,0:T(8,128)(2,1)}, ...), branch_computations={%region_0.0_spmd, %region_1.0_spmd} | conditional | bytes 8 | solution.py:565
  52.6 179.1 %routed_experts.3 = bf16[192,2048]{1,0:T(8,128)(2,1)S(1)} custom-call(bf16[192,2048]{1,0:T(8,128)(2,1)} %get-tuple-element.43.normed_ref, bf16[192,2048]{1,0:T(8,128)(2,1)S(1)} %get-tuple-element.44.hidden_ref, f32[192,128]{1,0:T(8,128)S(1)} %get-tuple-element.45.columns_ref, f32[8,256]{1,0:T(8,128)S(1)} %get-tuple-element.46.lanes_ref, ...), custom_call_target="tpu_custom_call" | custom-call | tf_op jit(solution)/shard_map/cond/branch_1_fun/routed_experts/pallas_call | solution.py:512
  231.8 0.9 copy.26
Async XLA Ops:
  2.4 1.1 copy-start
  3.5 1.1 copy-start.1
  4.7 1.1 copy-start.2
  5.8 1.1 copy-start.3
  6.9 1.1 copy-start.4
  8.1 0.7 copy-start.5
  8.8 0.7 copy-start.6
  9.5 0.7 copy-start.7
  10.2 42.3 %copy-start.8 = (bf16[1,2048,512]{2,1,0:T(8,128)(2,1)S(1)}, bf16[1,2048,512]{2,1,0:T(8,128)(2,1)}, u32[]{:S(2)}) copy-start(bf16[1,2048,512]{2,1,0:T(8,128)(2,1)} %param.29) | copy-start | bytes 6291460

commit v3 on v2

--- a/solution.py
+++ b/solution.py
@@ -15,6 +15,9 @@
 
 epsilon = 1e-06
 WIDTH = 256
+VMEM_LIMIT = 67043328
+DEPTH = 2
+WINDOW = 3
 USUAL = 80
 
 
@@ -28,9 +31,10 @@
 
 def mixer_kernel(
     sizes, limit, parts,
-    taps_ref, mix_gain_ref, expert_gain_ref, ids_ref, share_ref, scores_ref,
+    taps_hbm, mix_gain_hbm, expert_gain_hbm, ids_hbm, share_hbm, scores_hbm,
     outer_hbm, inner_hbm, input_hbm, weight_hbm, gate_hbm, residual_hbm,
     hidden_ref, normed_ref, columns_ref, lanes_ref, most_ref,
+    taps_ref, mix_gain_ref, expert_gain_ref, ids_v, share_v, scores_v,
     outer_v, inner_v, input_v, weight_v, gate_v, residual_v,
     products, mixed, own, far, far_in, near, near_in, tails, tail_in, table,
     mine, x_in, g_in, z_in, sent_x, sent_g,
@@ -53,7 +57,9 @@
         for i, (src, dst) in enumerate(
             (
                 (inner_hbm, inner_v), (input_hbm, input_v), (outer_hbm, outer_v),
-                (weight_hbm, weight_v), (gate_hbm, gate_v), (residual_hbm, residual_v),
+                (taps_hbm, taps_ref), (weight_hbm, weight_v), (ids_hbm, ids_v), (share_hbm, share_v),
+                (scores_hbm, scores_v), (gate_hbm, gate_v), (residual_hbm, residual_v),
+                (mix_gain_hbm, mix_gain_ref), (expert_gain_hbm, expert_gain_ref),
             )
         )
     ]
@@ -92,6 +98,7 @@
         at = slice(b * rows, (b + 1) * rows)
         products[pad + b * rows : pad + (b + 1) * rows, :] = inner_v[at, :].astype(f32) * input_v[at, :].astype(f32)
     loads[2].wait()
+    loads[3].wait()
     for b in reversed(range(xs)):
         if b == 0:
             tail_copy.wait_recv()
@@ -103,7 +110,7 @@
         conv = conv + taps_ref[1:2, :] * products[start + pad - 1 : start + pad - 1 + rows, :]
         conv = conv + taps_ref[2:3, :] * products[start + pad : start + pad + rows, :]
         mixed[start : start + rows, :] = (outer_v[start : start + rows, :].astype(f32) * conv).astype(bf)
-    loads[3].wait()
+    loads[4].wait()
 
     right, left = lax.rem(x + 1, xs), lax.rem(x + xs - 1, xs)
     ways = (right, left)
@@ -128,20 +135,39 @@
             device_id={X: ways[d]}, device_id_type=MESH,
         )
 
+    steps = [functools.partial(far_copy, t=t) for t in range(parts)]
+    steps += [lambda d, t=t: near_copy(d, 1 - d, t) for t in range(parts)]
+    steps += [lambda d, t=t: near_copy(d, d, t) for t in range(parts)]
+
     opposite = lax.rem(x + 2, xs)
     for h in range(2):
         far[h] = partial_of(opposite, h).astype(bf)
-        for t in range(parts):
-            far_copy(h, t).start()
+        for t in range(WINDOW):
+            steps[t](h).start()
     for d in range(2):
         near[d, 1 - d] = partial_of(ways[d], 1 - d).astype(bf)
-        for t in range(parts):
-            near_copy(d, 1 - d, t).start()
     for d in range(2):
         own[:, d * half : (d + 1) * half] = partial_of(ways[d], d)
 
-    tokens = ids_ref.shape[0]
-    expert = [ids_ref[:, k : k + 1].astype(f32) for k in range(2)]
+    def step(i):
+        for d in range(2):
+            steps[i](d).wait_recv()
+            if i < parts:
+                at = slice(i * piece, (i + 1) * piece)
+                near[d, d, at, :] = (own[at, d * half : (d + 1) * half] + far_in[d, at, :].astype(f32)).astype(bf)
+            if i + WINDOW < len(steps):
+                steps[i + WINDOW](d).start()
+
+    step(0)
+    tokens = ids_v.shape[1]
+    for load in loads[5:8]:
+        load.wait()
+    table[...] = jnp.zeros_like(table)
+    table[0:2, 0:tokens] = ids_v[...].astype(f32)
+    table[2:4, 0:tokens] = scores_v[...]
+    table[4:5, 0:tokens] = share_v[...]
+    given = jnp.transpose(table[...])[0:tokens, :]
+    expert = [given[:, k : k + 1] for k in range(2)]
     z_of = [jnp.floor((e + 0.5) / groups) for e in expert]
     lane = lax.broadcasted_iota(jnp.int32, (tokens, 128), 1).astype(f32)
     marks = [
@@ -172,7 +198,8 @@
 
     seen = [dot32(before, marks[0].astype(bf)), dot32(before, marks[1].astype(bf)) + first_sum]
     info = []
-    scores = [scores_ref[:, k : k + 1] for k in range(2)]
+    step(1)
+    scores = [given[:, 2 + k : 3 + k] for k in range(2)]
     top = jnp.maximum(scores[0], scores[1])
     powers = [jnp.exp(v - top) for v in scores]
     for k in range(2):
@@ -180,15 +207,15 @@
         rank = jnp.sum(jnp.where(lane < devices, hit, 0.0), axis=1, keepdims=True)
         place = jnp.sum(jnp.where(lane >= devices, hit, 0.0), axis=1, keepdims=True)
         slot = (expert[k] - groups * z_of[k]) * (zs * limit) + (z * limit).astype(f32) + rank
-        info.append((z_of[k], place, slot, share_ref[...] * (powers[k] / (powers[0] + powers[1]))))
+        info.append((z_of[k], place, slot, given[:, 4:5] * (powers[k] / (powers[0] + powers[1]))))
     column = jnp.zeros((tokens, 128), f32)
     for i in range(4):
         for k in range(2):
             column = column + jnp.where(lane == 2 * i + k, info[k][i], 0.0)
     columns_ref[...] = column
-    table[...] = jnp.zeros_like(table)
-    table[0:tokens, :] = column
-    lanes_ref[...] = jnp.transpose(table[...])[0:8, :]
+    spare = jnp.zeros((table.shape[1] - tokens, 128), f32)
+    lanes_ref[...] = jnp.transpose(jnp.concatenate([column, spare], axis=0))[0:8, :]
+    step(2)
 
     for flag in x_flags:
         flag.wait_recv()
@@ -198,12 +225,8 @@
     for flag in g_flags:
         flag.start()
 
-    for t in range(parts):
-        at = slice(t * piece, (t + 1) * piece)
-        for d in range(2):
-            far_copy(d, t).wait_recv()
-            near[d, d, at, :] = (own[at, d * half : (d + 1) * half] + far_in[d, at, :].astype(f32)).astype(bf)
-            near_copy(d, d, t).start()
+    for i in range(3, parts):
+        step(i)
     for h in range(2):
         own[:, h * half : (h + 1) * half] = partial_of(x, h)
 
@@ -215,13 +238,13 @@
     for flag in z_flags:
         flag.start()
 
-    loads[4].wait()
-    loads[5].wait()
+    for load in loads[8:]:
+        load.wait()
+    for i in range(parts, 2 * parts):
+        step(i)
     for t in range(parts):
         at = slice(t * piece, (t + 1) * piece)
-        for d in range(2):
-            for h in range(2):
-                near_copy(d, h, t).wait_recv()
+        step(2 * parts + t)
         sums = []
         for h in range(2):
             part = own[at, h * half : (h + 1) * half]
@@ -256,7 +279,7 @@
     rows, model = residual.shape
     half, parts, last = model // 2, 4, 16
     bf, f32 = jnp.bfloat16, jnp.float32
-    vmem, anywhere = pl.BlockSpec(memory_space=pltpu.VMEM), pl.BlockSpec(memory_space=pl.ANY)
+    vmem, anywhere = pl.BlockSpec(memory_space=pltpu.VMEM), pl.BlockSpec(memory_space=pltpu.HBM)
     dma = pltpu.SemaphoreType.DMA
     flag = (8, 128)
     return pl.pallas_call(
@@ -268,9 +291,11 @@
             jax.ShapeDtypeStruct((8, 256), f32),
             jax.ShapeDtypeStruct(flag, f32),
         ),
-        in_specs=[vmem] * 6 + [anywhere] * 6,
+        in_specs=[anywhere] * 12,
         out_specs=(vmem,) * 5,
         scratch_shapes=[
+            pltpu.VMEM(taps.shape, f32), pltpu.VMEM((1, model), f32), pltpu.VMEM((1, model), f32),
+            pltpu.VMEM((2, rows), jnp.int32), pltpu.VMEM((1, rows), f32), pltpu.VMEM((2, rows), f32),
             pltpu.VMEM(outer.shape, bf), pltpu.VMEM(inner.shape, bf), pltpu.VMEM(values.shape, bf),
             pltpu.VMEM(weight.shape, bf), pltpu.VMEM(gate.shape, bf), pltpu.VMEM(residual.shape, bf),
             pltpu.VMEM((length + 8, lanes), f32),
@@ -279,20 +304,20 @@
             pltpu.VMEM((2, rows, half), bf), pltpu.VMEM((2, rows, half), bf),
             pltpu.VMEM((2, 2, rows, half), bf), pltpu.VMEM((2, 2, rows, half), bf),
             pltpu.VMEM((2, last, lanes), bf), pltpu.VMEM((2, last, lanes), bf),
-            pltpu.VMEM((256, 128), f32),
+            pltpu.VMEM((128, 256), f32),
             pltpu.VMEM(flag, f32), pltpu.VMEM((xs - 1, *flag), f32),
             pltpu.VMEM((groups - 1, *flag), f32), pltpu.VMEM((zs - 1, *flag), f32),
             pltpu.VMEM(flag, f32), pltpu.VMEM(flag, f32),
-            dma((6,)), dma, dma,
+            dma((12,)), dma, dma,
             dma((2, parts)), dma((2, parts)), dma((2, 2, parts)), dma((2, 2, parts)),
             dma((xs - 1,)), dma((xs - 1,)), dma((groups - 1,)), dma((groups - 1,)), dma((zs - 1,)), dma((zs - 1,)),
         ],
         compiler_params=pltpu.CompilerParams(
-            collective_id=1, has_side_effects=True, vmem_limit_bytes=48 * 1024 * 1024
+            collective_id=1, has_side_effects=True, vmem_limit_bytes=VMEM_LIMIT
         ),
         name="mixer",
     )(
-        taps, mix_gain[None, :], expert_gain[None, :], ids, share[:, None], scores,
+        taps, mix_gain[None, :], expert_gain[None, :], ids.T, share[None, :], scores.T,
         outer, inner, values, weight, gate, residual,
     )
 
@@ -380,13 +405,14 @@
         hit = [place + float(j * cap) == r for r in row_of]
         pick_ref[j * cap : (j + 1) * cap, :] = jnp.where(hit[0] | hit[1], jnp.ones((), f32), jnp.zeros((), f32)).astype(bf)
 
-    @pl.loop(0, chunks)
-    def _(k):
+    def pick_rows(k):
         values = normed_ref[:, columns(k)]
-        for j in range(zs):
-            s1[k, j] = dot32(pick_ref[j * cap : (j + 1) * cap, :], values).astype(bf)
+        s1[k] = dot32(pick_ref[...], values).astype(bf).reshape(zs, cap, width)
+        r1[k, z] = s1[k, z]
+
+    for k in range(DEPTH):
+        pick_rows(k)
         start_all(z_sends, k, zs)
-        r1[k, z] = s1[k, z]
 
     for j in range(zs):
         hit = [place + float(j * cap) == r for r in row_of]
@@ -404,6 +430,11 @@
     whi_ref[...] = weigh.astype(bf)
     wlo_ref[...] = (weigh - whi_ref[...].astype(f32)).astype(bf)
     metar[z] = meta_ref[z]
+
+    @pl.loop(DEPTH, chunks)
+    def _(k):
+        pick_rows(k)
+
     for o in range(1, zs):
         m_copy(o).wait_recv()
     total = groups * slots
@@ -431,9 +462,17 @@
         @pl.when(k < chunks)
         def _():
             wait_recv_all(z_sends, k, zs)
+
+            @pl.when(k + DEPTH < chunks)
+            def _():
+                start_all(z_sends, k + DEPTH, zs)
+
             rows = r1[k].reshape(zs * cap, width)
-            for g in range(groups):
-                s2[k, g] = dot32(onehot[g * slots : (g + 1) * slots, :], rows).astype(bf)
+            for half in range(2):
+                at = slice(half * total // 2, (half + 1) * total // 2)
+                s2[k, half * groups // 2 : (half + 1) * groups // 2] = (
+                    dot32(onehot[at, :], rows).astype(bf).reshape(groups // 2, slots, width)
+                )
             start_all(g_sends, k, groups)
             r2[k, g_me] = s2[k, g_me]
 
@@ -457,30 +496,52 @@
 
     weights[2].wait()
 
-    @pl.loop(0, chunks)
+    def outputs_of(k):
+        down = down_v[:, columns(k)]
+        for half in range(2):
+            at = slice(half * total // 2, (half + 1) * total // 2)
+            o2[k, half * groups // 2 : (half + 1) * groups // 2] = (
+                dot32(act[at, :], down).astype(bf).reshape(groups // 2, slots, width)
+            )
+        b2[k, g_me] = o2[k, g_me]
+
+    for k in range(DEPTH):
+        outputs_of(k)
+        start_all(g_backs, k, groups)
+
+    @pl.loop(DEPTH, chunks)
     def _(k):
-        down = down_v[:, columns(k)]
-        for g in range(groups):
-            o2[k, g] = dot32(act[g * slots : (g + 1) * slots, :], down).astype(bf)
-        start_all(g_backs, k, groups)
-        b2[k, g_me] = o2[k, g_me]
-
-    @pl.loop(0, chunks)
+        outputs_of(k)
+
+    @pl.loop(0, chunks + DEPTH)
     def _(k):
-        wait_recv_all(g_backs, k, groups)
-        rows = b2[k].reshape(total, width)
-        for j in range(zs):
-            o1[k, j] = dot32(onehot_t[j * cap : (j + 1) * cap, :], rows).astype(bf)
-        start_all(z_backs, k, zs)
-        b1[k, z] = o1[k, z]
-
-    @pl.loop(0, chunks)
-    def _(k):
-        wait_recv_all(z_backs, k, zs)
-        rows = b1[k].reshape(zs * cap, width)
-        value = hidden_ref[:, columns(k)].astype(jnp.float32)
-        value = value + (dot32(whi_ref[...], rows) + dot32(wlo_ref[...], rows))
-        out_ref[:, columns(k)] = value.astype(bf)
+        @pl.when(k < chunks)
+        def _():
+            wait_recv_all(g_backs, k, groups)
+
+            @pl.when(k + DEPTH < chunks)
+            def _():
+                start_all(g_backs, k + DEPTH, groups)
+
+            rows = b2[k].reshape(total, width)
+            o1[k] = dot32(onehot_t[...], rows).astype(bf).reshape(zs, cap, width)
+            b1[k, z] = o1[k, z]
+
+        @pl.when(k >= DEPTH)
+        def _():
+            wait_recv_all(z_backs, k - DEPTH, zs)
+
+        @pl.when(k < chunks)
+        def _():
+            start_all(z_backs, k, zs)
+
+        @pl.when(k >= DEPTH)
+        def _():
+            b = k - DEPTH
+            rows = b1[b].reshape(zs * cap, width)
+            value = hidden_ref[:, columns(b)].astype(jnp.float32)
+            value = value + (dot32(whi_ref[...], rows) + dot32(wlo_ref[...], rows))
+            out_ref[:, columns(b)] = value.astype(bf)
 
     for o in range(1, zs):
         m_copy(o).wait_send()
@@ -504,7 +565,7 @@
     chunks = model // WIDTH
     units = gate.shape[1]
     bf = jnp.bfloat16
-    vmem, anywhere = pl.BlockSpec(memory_space=pltpu.VMEM), pl.BlockSpec(memory_space=pl.ANY)
+    vmem, anywhere = pl.BlockSpec(memory_space=pltpu.VMEM), pl.BlockSpec(memory_space=pltpu.HBM)
     z_block, g_block = (chunks, zs, cap, WIDTH), (chunks, groups, slots, WIDTH)
     z_sem, g_sem = pltpu.SemaphoreType.DMA((chunks, zs - 1)), pltpu.SemaphoreType.DMA((chunks, groups - 1))
     m_sem = pltpu.SemaphoreType.DMA((zs - 1,))
@@ -531,7 +592,7 @@
             pltpu.SemaphoreType.DMA((3,)),
         ],
         compiler_params=pltpu.CompilerParams(
-            collective_id=collective, has_side_effects=True, vmem_limit_bytes=60 * 1024 * 1024
+            collective_id=collective, has_side_effects=True, vmem_limit_bytes=VMEM_LIMIT
         ),
         name="routed_experts",
     )(normed, hidden, columns, lanes, gate, up, down)

time: 233 us -> 198 us (0.85)
  Pallas kernels: 220 us -> 194 us
  local copies, waits for them, and re-layouts: 11.5 us -> 3.28 us
    pallas_call x1, Pallas kernels: 179 us -> 151 us  [routed_experts(): pl.pallas_call(functools.partial(expert_kernel, zs, ys, cs, cap, slots),...]
    unnamed x21 -> x1, local copies, waits for them, and re-layouts: 10.2 us -> 2.09 us
where the time goes in v3:
time: 198 us
  Pallas kernels  194 us (98%)
  local copies, waits for them, and re-layouts  3.28 us (2%)
    pallas_call x1, Pallas kernels, routed_experts(): pl.pallas_call(functools.partial(expert_kernel, zs, ys, cs, cap, slots),...  151 us
    pallas_call x1, Pallas kernels, mixer(): pl.pallas_call(functools.partial(mixer_kernel, sizes, limit, parts), out_...  43.3 us

profile of v3, /device:TPU:1, one launch (start us, length us, event | category | flops | bytes accessed | tf_op | source)
XLA Modules:
  0.0 198.2 jit_solution(15654469853867043593)
XLA Ops:
  0.0 43.3 %mixer.1 = (bf16[192,2048]{1,0:T(8,128)(2,1)}, bf16[192,2048]{1,0:T(8,128)(2,1)}, f32[192,128]{1,0:T(8,128)}, f32[8,256]{1,0:T(8,128)}, f32[8,128]{1,0:T(8,128)}) custom-call(f32[3,512]{1,0:T(4,128)} %taps_hbm.1, f32[1,2048]{1,0:T(1,128)} %bitcast.15, f32[1,2048]{1,0:T(1,128)} %bitcast.16, s32[2,192]{1,0:T(2,128)} %bitcast.17, f32[1,192]{1,0:T(1,128)} %bitcast.19, ...), custom_call_target="tpu_custom_call" | custom-call | tf_op jit(solution)/shard_map/mixer/pallas_call | solution.py:285
  43.3 1.2 slice.3
  45.2 150.9 %conditional.1 = (bf16[192,2048]{1,0:T(8,128)(2,1)}) conditional(s32[]{:T(128)} %bitcast.5, (bf16[192,2048]{1,0:T(8,128)(2,1)}, bf16[192,2048]{1,0:T(8,128)(2,1)}, f32[192,128]{1,0:T(8,128)}, f32[8,256]{1,0:T(8,128)}, bf16[2048,512]{1,0:T(8,128)(2,1)}, /*index=5*/bf16[2048,512]{1,0:T(8,128)(2,1)}, bf16[512,2048]{1,0:T(8,128)(2,1)}) %tuple.20, ...), branch_computations={%region_0.0_spmd, %region_1.0_spmd} | conditional | bytes 8 | solution.py:626
  45.3 150.7 %routed_experts.3 = bf16[192,2048]{1,0:T(8,128)(2,1)} custom-call(bf16[192,2048]{1,0:T(8,128)(2,1)} %get-tuple-element.43.normed_ref, bf16[192,2048]{1,0:T(8,128)(2,1)} %get-tuple-element.44.hidden_ref, f32[192,128]{1,0:T(8,128)} %get-tuple-element.45.columns_ref, f32[8,256]{1,0:T(8,128)} %get-tuple-element.46.lanes_ref, ...), custom_call_target="tpu_custom_call" | custom-call | tf_op jit(solution)/shard_map/cond/branch_1_fun/routed_experts/pallas_call | solution.py:573
  196.1 2.1 %copy.21 = bf16[192,2048]{1,0:T(8,128)(2,1)} copy(bf16[192,2048]{1,0:T(8,128)(2,1)} %get-tuple-element.60) | data formatting | bytes 1572864

commit v4 on v3

--- a/solution.py
+++ b/solution.py
@@ -14,11 +14,11 @@
 MESH = pl.DeviceIdType.MESH
 
 epsilon = 1e-06
-WIDTH = 256
+WIDTH = 512
 VMEM_LIMIT = 67043328
 DEPTH = 2
 WINDOW = 3
-USUAL = 80
+USUAL = 40
 
 
 def rms_scale(values, gain):
@@ -170,18 +170,24 @@
     expert = [given[:, k : k + 1] for k in range(2)]
     z_of = [jnp.floor((e + 0.5) / groups) for e in expert]
     lane = lax.broadcasted_iota(jnp.int32, (tokens, 128), 1).astype(f32)
-    marks = [
-        jnp.where((e == lane) | (zz + devices == lane), jnp.ones((), f32), jnp.zeros((), f32))
-        for e, zz in zip(expert, z_of)
-    ]
     before = jnp.where(
         lax.broadcasted_iota(jnp.int32, (tokens, tokens), 1) < lax.broadcasted_iota(jnp.int32, (tokens, tokens), 0),
         jnp.ones((), f32), jnp.zeros((), f32),
     ).astype(bf)
-    first_sum = jnp.sum(marks[0], axis=0, keepdims=True)
-    most = first_sum + jnp.sum(marks[1], axis=0, keepdims=True)
-    most = jnp.where(lane[0:1, :] >= devices, most, jnp.zeros_like(most))
-    most = jnp.broadcast_to(jnp.max(most, axis=1, keepdims=True), (8, 128))
+
+    def ranks(labels):
+        marks = [jnp.where(label == lane, jnp.ones((), f32), jnp.zeros((), f32)) for label in labels]
+        firsts = jnp.sum(marks[0], axis=0, keepdims=True)
+        seen = [dot32(before, marks[0].astype(bf)), dot32(before, marks[1].astype(bf)) + firsts]
+        found = [jnp.sum(mark * s, axis=1, keepdims=True) for mark, s in zip(marks, seen)]
+        return found, jnp.max(firsts + jnp.sum(marks[1], axis=0, keepdims=True), axis=1, keepdims=True)
+
+    rank, _ = ranks(expert)
+    lower = [jnp.floor(r * 0.5) for r in rank]
+    parity = [r + e - 2.0 * jnp.floor((r + e) * 0.5) for r, e in zip(rank, expert)]
+    block = [h * zs + zz for h, zz in zip(parity, z_of)]
+    place, most = ranks(block)
+    most = jnp.broadcast_to(most, (8, 128))
     mine[...] = most
 
     def flag_copy(src, dst, send, recv, i, peer):
@@ -196,18 +202,14 @@
     for flag in x_flags:
         flag.start()
 
-    seen = [dot32(before, marks[0].astype(bf)), dot32(before, marks[1].astype(bf)) + first_sum]
     info = []
     step(1)
     scores = [given[:, 2 + k : 3 + k] for k in range(2)]
     top = jnp.maximum(scores[0], scores[1])
     powers = [jnp.exp(v - top) for v in scores]
     for k in range(2):
-        hit = marks[k] * seen[k]
-        rank = jnp.sum(jnp.where(lane < devices, hit, 0.0), axis=1, keepdims=True)
-        place = jnp.sum(jnp.where(lane >= devices, hit, 0.0), axis=1, keepdims=True)
-        slot = (expert[k] - groups * z_of[k]) * (zs * limit) + (z * limit).astype(f32) + rank
-        info.append((z_of[k], place, slot, given[:, 4:5] * (powers[k] / (powers[0] + powers[1]))))
+        slot = (expert[k] - groups * z_of[k]) * (zs * limit / 2) + (z * limit).astype(f32) * 0.5 + lower[k]
+        info.append((block[k], place[k], slot, given[:, 4:5] * (powers[k] / (powers[0] + powers[1]))))
     column = jnp.zeros((tokens, 128), f32)
     for i in range(4):
         for k in range(2):
@@ -326,15 +328,23 @@
     zs, ys, cs, cap, slots,
     normed_ref, hidden_ref, columns_ref, lanes_ref, gate_hbm, up_hbm, down_hbm,
     out_ref,
-    pick_ref, meta_ref, whi_ref, wlo_ref, s1, r1, s2, r2, o2, b2, o1, b1, metar, onehot_t, onehot, acc, act, gate_v, up_v, down_v,
+    pick, weigh, meta, s1, r1, s2, r2, o2, b2, o1, b1, metar, onehot_t, onehot, acc, act, partial,
+    gate_v, up_v, down_v,
     z_send, z_recv, g_send, g_recv, bg_send, bg_recv, bz_send, bz_recv, m_send, m_recv, w_sem,
 ):
     z, y, c = lax.axis_index(Z), lax.axis_index(Y), lax.axis_index(CORE)
     groups = ys * cs
     g_me = y * cs + c
     chunks = s1.shape[0]
-    width = s1.shape[3]
-    bf = jnp.bfloat16
+    each = chunks // 2
+    side = s1.shape[3]
+    width = 2 * side
+    tokens = normed_ref.shape[0]
+    rows = zs * cap
+    padded = onehot_t.shape[1]
+    total = groups * slots
+    bf, f32 = jnp.bfloat16, jnp.float32
+    one, zero = jnp.ones((), f32), jnp.zeros((), f32)
 
     weights = [
         pltpu.make_async_copy(src, dst, w_sem.at[i])
@@ -357,7 +367,6 @@
         pl.semaphore_signal(barrier, inc=1, device_id={Z: z_peer(o)}, device_id_type=MESH)
     for o in range(1, groups):
         pl.semaphore_signal(barrier, inc=1, device_id=g_device(g_peer(o)), device_id_type=MESH)
-    pl.semaphore_wait(barrier, zs + groups - 2)
 
     def z_copy(src, dst, send, recv, k, o):
         return pltpu.make_async_remote_copy(
@@ -375,7 +384,7 @@
 
     def m_copy(o):
         return pltpu.make_async_remote_copy(
-            src_ref=meta_ref.at[z_peer(o)], dst_ref=metar.at[z],
+            src_ref=meta.at[z_peer(o)], dst_ref=metar.at[z],
             send_sem=m_send.at[o - 1], recv_sem=m_recv.at[o - 1],
             device_id={Z: z_peer(o)}, device_id_type=MESH,
         )
@@ -393,43 +402,76 @@
         for o in range(1, count):
             copies(k, o).wait_recv()
 
+    def half_of(k):
+        return lax.div(k, each)
+
     def columns(k):
-        return pl.ds(pl.multiple_of(k * width, width), width)
-
-    f32 = jnp.float32
-    tokens = normed_ref.shape[0]
-    row_of = [lanes_ref[k : k + 1, 0:tokens] * cap + lanes_ref[2 + k : 3 + k, 0:tokens] for k in range(2)]
+        return pl.ds(pl.multiple_of(lax.rem(k, each) * width, width), width)
+
+    def fold(value):
+        parts = []
+        for j in range(zs):
+            at = slice(j * cap, (j + 1) * cap)
+            parts.append(jnp.concatenate([value[at, :side], value[at, side:]], axis=0)[None])
+        return jnp.concatenate(parts, axis=0).astype(bf)
+
+    def unfold(ref, k):
+        value = ref[k].astype(f32).reshape(zs, 2, cap, side)
+        sides = []
+        for i in range(2):
+            flat = value[:, i].reshape(rows, side)
+            if padded > rows:
+                flat = jnp.concatenate([flat, jnp.zeros((padded - rows, side), f32)], axis=0)
+            sides.append(flat.astype(bf))
+        return sides
+
+    def row_of(block, place, h):
+        inside = (block >= float(h * zs)) & (block < float((h + 1) * zs))
+        return jnp.where(inside, (block - float(h * zs)) * cap + place, -1.0)
+
+    lane_rows = [
+        [row_of(lanes_ref[k : k + 1, 0:tokens], lanes_ref[2 + k : 3 + k, 0:tokens], h) for k in range(2)]
+        for h in range(2)
+    ]
     slot_of = [lanes_ref[4 + k : 5 + k, 0:tokens] + 1.0 for k in range(2)]
-    place = lax.broadcasted_iota(jnp.int32, (cap, tokens), 0).astype(f32)
-    for j in range(zs):
-        hit = [place + float(j * cap) == r for r in row_of]
-        pick_ref[j * cap : (j + 1) * cap, :] = jnp.where(hit[0] | hit[1], jnp.ones((), f32), jnp.zeros((), f32)).astype(bf)
+    numbers = lax.broadcasted_iota(jnp.int32, (padded, tokens), 0).astype(f32)
+    for h in range(2):
+        hit = [numbers == r for r in lane_rows[h]]
+        pick[h] = jnp.where(hit[0] | hit[1], one, zero).astype(bf)
 
     def pick_rows(k):
-        values = normed_ref[:, columns(k)]
-        s1[k] = dot32(pick_ref[...], values).astype(bf).reshape(zs, cap, width)
+        value = dot32(pick[half_of(k)], normed_ref[:, columns(k)])
+        s1[k] = fold(value)
         r1[k, z] = s1[k, z]
 
+    pl.semaphore_wait(barrier, zs + groups - 2)
     for k in range(DEPTH):
         pick_rows(k)
         start_all(z_sends, k, zs)
 
+    place = lax.broadcasted_iota(jnp.int32, (cap, tokens), 0).astype(f32)
+    blank = jnp.full((128 - cap, 128), -1.0, f32)
+    spot = lax.broadcasted_iota(jnp.int32, (128, 128), 1).astype(f32)
     for j in range(zs):
-        hit = [place + float(j * cap) == r for r in row_of]
-        found = jnp.where(hit[0], slot_of[0], 0.0) + jnp.where(hit[1], slot_of[1], 0.0)
-        found = jnp.broadcast_to(jnp.sum(found, axis=1, keepdims=True) - 1.0, (cap, 128))
-        found = jnp.concatenate([found, jnp.full((128 - cap, 128), -1.0, f32)], axis=0)
-        meta_ref[j] = jnp.transpose(found)[0:8, :]
+        both = jnp.zeros((128, 128), f32)
+        for h in range(2):
+            hit = [place + float(j * cap) == r for r in lane_rows[h]]
+            found = jnp.where(hit[0], slot_of[0], 0.0) + jnp.where(hit[1], slot_of[1], 0.0)
+            found = jnp.broadcast_to(jnp.sum(found, axis=1, keepdims=True) - 1.0, (cap, 128))
+            both = jnp.where(spot == float(h), jnp.concatenate([found, blank], axis=0), both)
+        meta[j] = jnp.transpose(both)[0:8, :]
     for o in range(1, zs):
         m_copy(o).start()
-    row_lane = lax.broadcasted_iota(jnp.int32, (tokens, zs * cap), 1).astype(f32)
-    weigh = jnp.zeros((tokens, zs * cap), f32)
-    for k in range(2):
-        row = columns_ref[:, k : k + 1] * cap + columns_ref[:, 2 + k : 3 + k]
-        weigh = weigh + jnp.where(row == row_lane, columns_ref[:, 6 + k : 7 + k], 0.0)
-    whi_ref[...] = weigh.astype(bf)
-    wlo_ref[...] = (weigh - whi_ref[...].astype(f32)).astype(bf)
-    metar[z] = meta_ref[z]
+    row_lane = lax.broadcasted_iota(jnp.int32, (tokens, padded), 1).astype(f32)
+    for h in range(2):
+        weight = jnp.zeros((tokens, padded), f32)
+        for k in range(2):
+            row = row_of(columns_ref[:, k : k + 1], columns_ref[:, 2 + k : 3 + k], h)
+            weight = weight + jnp.where(row == row_lane, columns_ref[:, 6 + k : 7 + k], 0.0)
+        high = weight.astype(bf)
+        weigh[h, 0] = high
+        weigh[h, 1] = (weight - high.astype(f32)).astype(bf)
+    metar[z] = meta[z]
 
     @pl.loop(DEPTH, chunks)
     def _(k):
@@ -437,111 +479,102 @@
 
     for o in range(1, zs):
         m_copy(o).wait_recv()
-    total = groups * slots
-    places = lax.broadcasted_iota(jnp.int32, (cap, total), 1).astype(jnp.float32)
-
-    @pl.loop(0, zs)
-    def _(j):
-        where = jnp.transpose(metar[j])[:cap, 0:1]
-        onehot_t[pl.ds(pl.multiple_of(j * cap, 16), cap), :] = jnp.where(
-            where == places, jnp.ones((), jnp.float32), jnp.zeros((), jnp.float32)
-        ).astype(bf)
-
-    @pl.loop(0, zs * cap // 128)
-    def _(j):
-        rows = pl.ds(pl.multiple_of(j * 128, 128), 128)
-        onehot[:, rows] = jnp.transpose(onehot_t[rows, :].astype(jnp.float32)).astype(bf)
+    places = lax.broadcasted_iota(jnp.int32, (cap, total), 1).astype(f32)
+    for h in range(2):
+        blocks = []
+        for j in range(zs):
+            where = jnp.transpose(metar[j])[:cap, h : h + 1]
+            blocks.append(jnp.where(where == places, one, zero))
+        if padded > rows:
+            blocks.append(jnp.zeros((padded - rows, total), f32))
+        table = jnp.concatenate(blocks, axis=0)
+        onehot_t[h] = table.astype(bf)
+        onehot[h] = jnp.transpose(table).astype(bf)
 
     weights[0].wait()
     weights[1].wait()
+    weights[2].wait()
     acc[...] = jnp.zeros_like(acc)
-    hidden_units = gate_v.shape[1]
-
-    @pl.loop(0, chunks + 1)
-    def _(k):
-        @pl.when(k < chunks)
-        def _():
-            wait_recv_all(z_sends, k, zs)
-
-            @pl.when(k + DEPTH < chunks)
-            def _():
-                start_all(z_sends, k + DEPTH, zs)
-
-            rows = r1[k].reshape(zs * cap, width)
-            for half in range(2):
-                at = slice(half * total // 2, (half + 1) * total // 2)
-                s2[k, half * groups // 2 : (half + 1) * groups // 2] = (
-                    dot32(onehot[at, :], rows).astype(bf).reshape(groups // 2, slots, width)
-                )
-            start_all(g_sends, k, groups)
-            r2[k, g_me] = s2[k, g_me]
-
-        @pl.when(k >= 1)
-        def _():
-            b = k - 1
-            wait_recv_all(g_sends, b, groups)
-            ks = pl.ds(pl.multiple_of(b * width, width), width)
-            for half in range(2):
-                rows = r2[b, half * groups // 2 : (half + 1) * groups // 2].reshape(total // 2, width)
-                at = slice(half * total // 2, (half + 1) * total // 2)
-                acc[at, :hidden_units] += dot32(rows, gate_v[ks, :])
-                acc[at, hidden_units:] += dot32(rows, up_v[ks, :])
-
-    @pl.loop(0, groups)
-    def _(g):
-        at = pl.ds(pl.multiple_of(g * slots, slots), slots)
-        first = acc[at, :hidden_units]
-        second = acc[at, hidden_units:]
-        act[at, :] = (first / (1.0 + jnp.exp(-first)) * second).astype(bf)
-
-    weights[2].wait()
-
-    def outputs_of(k):
-        down = down_v[:, columns(k)]
-        for half in range(2):
-            at = slice(half * total // 2, (half + 1) * total // 2)
-            o2[k, half * groups // 2 : (half + 1) * groups // 2] = (
-                dot32(act[at, :], down).astype(bf).reshape(groups // 2, slots, width)
-            )
-        b2[k, g_me] = o2[k, g_me]
-
-    for k in range(DEPTH):
-        outputs_of(k)
-        start_all(g_backs, k, groups)
-
-    @pl.loop(DEPTH, chunks)
-    def _(k):
-        outputs_of(k)
-
-    @pl.loop(0, chunks + DEPTH)
-    def _(k):
-        @pl.when(k < chunks)
-        def _():
+    units = gate_v.shape[1]
+
+    @pl.loop(0, 2 * chunks)
+    def _(t):
+        @pl.when(t < chunks)
+        def _():
+            wait_recv_all(z_sends, t, zs)
+
+        @pl.when(t >= chunks)
+        def _():
+            wait_recv_all(z_backs, t - chunks, zs)
+
+        @pl.when(t + DEPTH < chunks)
+        def _():
+            start_all(z_sends, t + DEPTH, zs)
+
+        @pl.when((t + DEPTH >= chunks) & (t + DEPTH < 2 * chunks))
+        def _():
+            start_all(z_backs, t + DEPTH - chunks, zs)
+
+        @pl.when(t < chunks)
+        def _():
+            sides = unfold(r1, t)
+            for i in range(2):
+                value = dot32(onehot[half_of(t)], sides[i]).astype(bf)
+                s2[t, :, :, i * side : (i + 1) * side] = value.reshape(groups, slots, side)
+            start_all(g_sends, t, groups)
+            r2[t, g_me] = s2[t, g_me]
+
+        @pl.when((t >= 1) & (t <= chunks))
+        def _():
+            k = t - 1
+            wait_recv_all(g_sends, k, groups)
+            values = r2[k].reshape(total, width)
+            h = half_of(k)
+            acc[h, :, :units] += dot32(values, gate_v[columns(k), :])
+            acc[h, :, units:] += dot32(values, up_v[columns(k), :])
+
+        @pl.when((t == each) | (t == chunks))
+        def _():
+            h = half_of(t - 1)
+            first = acc[h, :, :units]
+            act[...] = (first / (1.0 + jnp.exp(-first)) * acc[h, :, units:]).astype(bf)
+            for i in range(each):
+                k = h * each + i
+                value = dot32(act[...], down_v[:, i * width : (i + 1) * width]).astype(bf)
+                o2[k] = value.reshape(groups, slots, width)
+                b2[k, g_me] = o2[k, g_me]
+                if i < DEPTH:
+                    start_all(g_backs, k, groups)
+
+        @pl.when((t > each) & (t <= each + chunks))
+        def _():
+            k = t - each - 1
             wait_recv_all(g_backs, k, groups)
 
-            @pl.when(k + DEPTH < chunks)
+            @pl.when(lax.rem(k, each) + DEPTH < each)
             def _():
                 start_all(g_backs, k + DEPTH, groups)
 
-            rows = b2[k].reshape(total, width)
-            o1[k] = dot32(onehot_t[...], rows).astype(bf).reshape(zs, cap, width)
+            value = dot32(onehot_t[half_of(k)], b2[k].reshape(total, width))
+            o1[k] = fold(value)
             b1[k, z] = o1[k, z]
 
-        @pl.when(k >= DEPTH)
-        def _():
-            wait_recv_all(z_backs, k - DEPTH, zs)
-
-        @pl.when(k < chunks)
-        def _():
-            start_all(z_backs, k, zs)
-
-        @pl.when(k >= DEPTH)
-        def _():
-            b = k - DEPTH
-            rows = b1[b].reshape(zs * cap, width)
-            value = hidden_ref[:, columns(b)].astype(jnp.float32)
-            value = value + (dot32(whi_ref[...], rows) + dot32(wlo_ref[...], rows))
-            out_ref[:, columns(b)] = value.astype(bf)
+        @pl.when(t >= chunks)
+        def _():
+            k = t - chunks
+            h = half_of(k)
+            sides = unfold(b1, k)
+            for i in range(2):
+                at = pl.ds(pl.multiple_of(lax.rem(k, each) * width + i * side, side), side)
+                value = dot32(weigh[h, 0], sides[i]) + dot32(weigh[h, 1], sides[i])
+
+                @pl.when(h == 0)
+                def _():
+                    partial[:, at] = hidden_ref[:, at].astype(f32) + value
+
+                @pl.when(h == 1)
+                def _():
+                    out_ref[:, at] = (partial[:, at] + value).astype(bf)
 
     for o in range(1, zs):
         m_copy(o).wait_send()
@@ -560,15 +593,15 @@
     zs, ys, cs = lax.axis_size(Z), lax.axis_size(Y), lax.axis_size(CORE)
     groups = ys * cs
     tokens, model = normed.shape
-    slots = zs * limit
-    rows = zs * cap
-    chunks = model // WIDTH
+    slots = zs * limit // 2
+    padded = -(-zs * cap // 128) * 128
+    chunks = 2 * model // WIDTH
     units = gate.shape[1]
-    bf = jnp.bfloat16
+    bf, f32 = jnp.bfloat16, jnp.float32
     vmem, anywhere = pl.BlockSpec(memory_space=pltpu.VMEM), pl.BlockSpec(memory_space=pltpu.HBM)
-    z_block, g_block = (chunks, zs, cap, WIDTH), (chunks, groups, slots, WIDTH)
-    z_sem, g_sem = pltpu.SemaphoreType.DMA((chunks, zs - 1)), pltpu.SemaphoreType.DMA((chunks, groups - 1))
-    m_sem = pltpu.SemaphoreType.DMA((zs - 1,))
+    z_block, g_block = (chunks, zs, 2 * cap, WIDTH // 2), (chunks, groups, slots, WIDTH)
+    dma = pltpu.SemaphoreType.DMA
+    z_sem, g_sem, m_sem = dma((chunks, zs - 1)), dma((chunks, groups - 1)), dma((zs - 1,))
     total = groups * slots
     return pl.pallas_call(
         functools.partial(expert_kernel, zs, ys, cs, cap, slots),
@@ -576,20 +609,21 @@
         in_specs=[vmem] * 4 + [anywhere] * 3,
         out_specs=vmem,
         scratch_shapes=[
-            pltpu.VMEM((rows, tokens), bf), pltpu.VMEM((zs, 8, 128), jnp.float32),
-            pltpu.VMEM((tokens, rows), bf), pltpu.VMEM((tokens, rows), bf),
+            pltpu.VMEM((2, padded, tokens), bf), pltpu.VMEM((2, 2, tokens, padded), bf),
+            pltpu.VMEM((zs, 8, 128), f32),
             pltpu.VMEM(z_block, bf), pltpu.VMEM(z_block, bf),
             pltpu.VMEM(g_block, bf), pltpu.VMEM(g_block, bf),
             pltpu.VMEM(g_block, bf), pltpu.VMEM(g_block, bf),
             pltpu.VMEM(z_block, bf), pltpu.VMEM(z_block, bf),
-            pltpu.VMEM((zs, 8, 128), jnp.float32),
-            pltpu.VMEM((rows, total), bf),
-            pltpu.VMEM((total, rows), bf),
-            pltpu.VMEM((total, 2 * units), jnp.float32),
+            pltpu.VMEM((zs, 8, 128), f32),
+            pltpu.VMEM((2, padded, total), bf),
+            pltpu.VMEM((2, total, padded), bf),
+            pltpu.VMEM((2, total, 2 * units), f32),
             pltpu.VMEM((total, units), bf),
+            pltpu.VMEM((tokens, model), f32),
             pltpu.VMEM(gate.shape, bf), pltpu.VMEM(up.shape, bf), pltpu.VMEM(down.shape, bf),
             z_sem, z_sem, g_sem, g_sem, g_sem, g_sem, z_sem, z_sem, m_sem, m_sem,
-            pltpu.SemaphoreType.DMA((3,)),
+            dma((3,)),
         ],
         compiler_params=pltpu.CompilerParams(
             collective_id=collective, has_side_effects=True, vmem_limit_bytes=VMEM_LIMIT
@@ -616,7 +650,7 @@
     down_experts,
 ):
     limit = 2 * expert_ids.shape[1] * residual.shape[0] // (lax.axis_size(SP) * gate_experts.shape[0])
-    worst = limit * lax.axis_size(Y) * lax.axis_size(CORE)
+    worst = limit * lax.axis_size(Y) * lax.axis_size(CORE) // 2
     hidden, normed, columns, lanes, most = mixer(
         conv_outer, conv_inner, conv_input, conv_taps, out_weight, mix_gate, residual, mix_gain, expert_gain,
         expert_ids, group_share, pair_scores, limit,

time: 198 us -> 179 us (0.904)
  Pallas kernels: 194 us -> 175 us
    pallas_call x1, Pallas kernels: 151 us -> 131 us  [routed_experts(): pl.pallas_call(functools.partial(expert_kernel, zs, ys, cs, cap, slots),...]
where the time goes in v4:
time: 179 us
  Pallas kernels  175 us (98%)
  local copies, waits for them, and re-layouts  3.28 us (2%)
    pallas_call x1, Pallas kernels, routed_experts(): pl.pallas_call(functools.partial(expert_kernel, zs, ys, cs, cap, slots),...  131 us
    pallas_call x1, Pallas kernels, mixer(): pl.pallas_call(functools.partial(mixer_kernel, sizes, limit, parts), out_...  43.3 us

profile of v4, /device:TPU:1, one launch (start us, length us, event | category | flops | bytes accessed | tf_op | source)
XLA Modules:
  0.0 178.9 jit_solution(8418443533917858588)
XLA Ops:
  0.0 43.3 %mixer.1 = (bf16[192,2048]{1,0:T(8,128)(2,1)}, bf16[192,2048]{1,0:T(8,128)(2,1)}, f32[192,128]{1,0:T(8,128)}, f32[8,256]{1,0:T(8,128)}, f32[8,128]{1,0:T(8,128)}) custom-call(f32[3,512]{1,0:T(4,128)} %taps_hbm.1, f32[1,2048]{1,0:T(1,128)} %bitcast.15, f32[1,2048]{1,0:T(1,128)} %bitcast.16, s32[2,192]{1,0:T(2,128)} %bitcast.17, f32[1,192]{1,0:T(1,128)} %bitcast.19, ...), custom_call_target="tpu_custom_call" | custom-call | tf_op jit(solution)/shard_map/mixer/pallas_call | solution.py:287
  43.3 1.2 slice.3
  45.2 131.7 %conditional.1 = (bf16[192,2048]{1,0:T(8,128)(2,1)}) conditional(s32[]{:T(128)} %bitcast.5, (bf16[192,2048]{1,0:T(8,128)(2,1)}, bf16[192,2048]{1,0:T(8,128)(2,1)}, f32[192,128]{1,0:T(8,128)}, f32[8,256]{1,0:T(8,128)}, bf16[2048,512]{1,0:T(8,128)(2,1)}, /*index=5*/bf16[2048,512]{1,0:T(8,128)(2,1)}, bf16[512,2048]{1,0:T(8,128)(2,1)}) %tuple.20, ...), branch_computations={%region_0.0_spmd, %region_1.0_spmd} | conditional | bytes 8 | solution.py:660
  45.3 131.5 %routed_experts.3 = bf16[192,2048]{1,0:T(8,128)(2,1)} custom-call(bf16[192,2048]{1,0:T(8,128)(2,1)} %get-tuple-element.43.normed_ref, bf16[192,2048]{1,0:T(8,128)(2,1)} %get-tuple-element.44.hidden_ref, f32[192,128]{1,0:T(8,128)} %get-tuple-element.45.columns_ref, f32[8,256]{1,0:T(8,128)} %get-tuple-element.46.lanes_ref, ...), custom_call_target="tpu_custom_call" | custom-call | tf_op jit(solution)/shard_map/cond/branch_1_fun/routed_experts/pallas_call | solution.py:606
  176.8 2.1 %copy.21 = bf16[192,2048]{1,0:T(8,128)(2,1)} copy(bf16[192,2048]{1,0:T(8,128)(2,1)} %get-tuple-element.60) | data formatting | bytes 1572864

commit v5 on v4

--- a/solution.py
+++ b/solution.py
@@ -18,7 +18,7 @@
 VMEM_LIMIT = 67043328
 DEPTH = 2
 WINDOW = 3
-USUAL = 40
+USUAL = (36, 40)
 
 
 def rms_scale(values, gain):
@@ -86,37 +86,34 @@
     last = tails.shape[1]
     tails[0] = inner_v[length - last :, :]
     tails[1] = input_v[length - last :, :]
-    pl.semaphore_wait(barrier, len(everyone))
     tail_copy = pltpu.make_async_remote_copy(
         src_ref=tails, dst_ref=tail_in, send_sem=t_send, recv_sem=t_recv,
         device_id=sp_device(following), device_id_type=MESH,
     )
-    tail_copy.start()
 
     pad = 8
+    products[0:pad, :] = jnp.zeros((pad, lanes), f32)
     for b in range(xs):
         at = slice(b * rows, (b + 1) * rows)
         products[pad + b * rows : pad + (b + 1) * rows, :] = inner_v[at, :].astype(f32) * input_v[at, :].astype(f32)
     loads[2].wait()
     loads[3].wait()
-    for b in reversed(range(xs)):
-        if b == 0:
-            tail_copy.wait_recv()
-            earlier = tail_in[0].astype(f32) * tail_in[1].astype(f32)
-            earlier = jnp.where(me == 0, jnp.zeros_like(earlier), earlier)
-            products[0:pad, :] = earlier[last - pad :, :]
-        start = b * rows
-        conv = taps_ref[0:1, :] * products[start + pad - 2 : start + pad - 2 + rows, :]
-        conv = conv + taps_ref[1:2, :] * products[start + pad - 1 : start + pad - 1 + rows, :]
-        conv = conv + taps_ref[2:3, :] * products[start + pad : start + pad + rows, :]
-        mixed[start : start + rows, :] = (outer_v[start : start + rows, :].astype(f32) * conv).astype(bf)
+
+    def convolve(start, count):
+        conv = taps_ref[0:1, :] * products[start + pad - 2 : start + pad - 2 + count, :]
+        conv = conv + taps_ref[1:2, :] * products[start + pad - 1 : start + pad - 1 + count, :]
+        conv = conv + taps_ref[2:3, :] * products[start + pad : start + pad + count, :]
+        mixed[start : start + count, :] = (outer_v[start : start + count, :].astype(f32) * conv).astype(bf)
+
+    for b in range(xs):
+        convolve(b * rows, rows)
     loads[4].wait()
 
     right, left = lax.rem(x + 1, xs), lax.rem(x + xs - 1, xs)
     ways = (right, left)
 
-    def partial_of(owner, h):
-        block = mixed[pl.ds(pl.multiple_of(owner * rows, 16), rows), :]
+    def partial_of(owner, h, start=0, count=rows):
+        block = mixed[pl.ds(pl.multiple_of(owner * rows + start, 16), count), :]
         return dot32(block, weight_v[:, h * half : (h + 1) * half])
 
     def far_copy(h, t):
@@ -135,15 +132,26 @@
             device_id={X: ways[d]}, device_id_type=MESH,
         )
 
-    steps = [functools.partial(far_copy, t=t) for t in range(parts)]
-    steps += [lambda d, t=t: near_copy(d, 1 - d, t) for t in range(parts)]
-    steps += [lambda d, t=t: near_copy(d, d, t) for t in range(parts)]
+    order = [*range(1, parts), 0]
+    steps = [functools.partial(far_copy, t=t) for t in order]
+    steps += [lambda d, t=t: near_copy(d, 1 - d, t) for t in order]
+    steps += [lambda d, t=t: near_copy(d, d, t) for t in order]
 
     opposite = lax.rem(x + 2, xs)
     for h in range(2):
-        far[h] = partial_of(opposite, h).astype(bf)
-        for t in range(WINDOW):
-            steps[t](h).start()
+        far[h, piece:, :] = partial_of(opposite, h, piece, rows - piece).astype(bf)
+    pl.semaphore_wait(barrier, len(everyone))
+    tail_copy.start()
+    for i in range(WINDOW):
+        for h in range(2):
+            steps[i](h).start()
+    tail_copy.wait_recv()
+    earlier = tail_in[0].astype(f32) * tail_in[1].astype(f32)
+    earlier = jnp.where(me == 0, jnp.zeros_like(earlier), earlier)
+    products[0:pad, :] = earlier[last - pad :, :]
+    convolve(0, last)
+    for h in range(2):
+        far[h, :piece, :] = partial_of(opposite, h, 0, piece).astype(bf)
     for d in range(2):
         near[d, 1 - d] = partial_of(ways[d], 1 - d).astype(bf)
     for d in range(2):
@@ -153,7 +161,7 @@
         for d in range(2):
             steps[i](d).wait_recv()
             if i < parts:
-                at = slice(i * piece, (i + 1) * piece)
+                at = slice(order[i] * piece, (order[i] + 1) * piece)
                 near[d, d, at, :] = (own[at, d * half : (d + 1) * half] + far_in[d, at, :].astype(f32)).astype(bf)
             if i + WINDOW < len(steps):
                 steps[i + WINDOW](d).start()
@@ -244,9 +252,9 @@
         load.wait()
     for i in range(parts, 2 * parts):
         step(i)
-    for t in range(parts):
+    for i, t in enumerate(order):
         at = slice(t * piece, (t + 1) * piece)
-        step(2 * parts + t)
+        step(2 * parts + i)
         sums = []
         for h in range(2):
             part = own[at, h * half : (h + 1) * half]
@@ -337,10 +345,11 @@
     g_me = y * cs + c
     chunks = s1.shape[0]
     each = chunks // 2
-    side = s1.shape[3]
-    width = 2 * side
+    high = -(-cap // 8) * 8
+    width = s2.shape[3]
+    side = width // 2
     tokens = normed_ref.shape[0]
-    rows = zs * cap
+    rows = zs * high
     padded = onehot_t.shape[1]
     total = groups * slots
     bf, f32 = jnp.bfloat16, jnp.float32
@@ -409,25 +418,36 @@
         return pl.ds(pl.multiple_of(lax.rem(k, each) * width, width), width)
 
     def fold(value):
-        parts = []
+        value = value.reshape(zs, high, width)
+        if high == cap:
+            return value.astype(bf)
+        whole = high - 8
+        left, right = value[:, :, :side], value[:, :, side:]
+        blocks = []
         for j in range(zs):
-            at = slice(j * cap, (j + 1) * cap)
-            parts.append(jnp.concatenate([value[at, :side], value[at, side:]], axis=0)[None])
-        return jnp.concatenate(parts, axis=0).astype(bf)
+            ends = left[j, whole:] + pltpu.roll(right[j, whole:], 4, 0)
+            blocks.append(jnp.concatenate([left[j, :whole], right[j, :whole], ends], axis=0)[None])
+        return jnp.concatenate(blocks, axis=0).astype(bf)
 
     def unfold(ref, k):
-        value = ref[k].astype(f32).reshape(zs, 2, cap, side)
-        sides = []
-        for i in range(2):
-            flat = value[:, i].reshape(rows, side)
-            if padded > rows:
-                flat = jnp.concatenate([flat, jnp.zeros((padded - rows, side), f32)], axis=0)
-            sides.append(flat.astype(bf))
-        return sides
+        value = ref[k].astype(f32)
+        if high == cap:
+            blocks = [value.reshape(rows, width)]
+        else:
+            whole = high - 8
+            blocks = []
+            for j in range(zs):
+                ends = value[j, 2 * whole :]
+                left = jnp.concatenate([value[j, :whole], ends], axis=0)
+                right = jnp.concatenate([value[j, whole : 2 * whole], pltpu.roll(ends, 4, 0)], axis=0)
+                blocks.append(jnp.concatenate([left, right], axis=1))
+        if padded > rows:
+            blocks.append(jnp.zeros((padded - rows, width), f32))
+        return jnp.concatenate(blocks, axis=0).astype(bf)
 
     def row_of(block, place, h):
         inside = (block >= float(h * zs)) & (block < float((h + 1) * zs))
-        return jnp.where(inside, (block - float(h * zs)) * cap + place, -1.0)
+        return jnp.where(inside, (block - float(h * zs)) * high + place, -1.0)
 
     lane_rows = [
         [row_of(lanes_ref[k : k + 1, 0:tokens], lanes_ref[2 + k : 3 + k, 0:tokens], h) for k in range(2)]
@@ -441,7 +461,7 @@
 
     def pick_rows(k):
         value = dot32(pick[half_of(k)], normed_ref[:, columns(k)])
-        s1[k] = fold(value)
+        s1[k] = fold(value[:rows])
         r1[k, z] = s1[k, z]
 
     pl.semaphore_wait(barrier, zs + groups - 2)
@@ -449,15 +469,15 @@
         pick_rows(k)
         start_all(z_sends, k, zs)
 
-    place = lax.broadcasted_iota(jnp.int32, (cap, tokens), 0).astype(f32)
-    blank = jnp.full((128 - cap, 128), -1.0, f32)
+    place = lax.broadcasted_iota(jnp.int32, (high, tokens), 0).astype(f32)
+    blank = jnp.full((128 - high, 128), -1.0, f32)
     spot = lax.broadcasted_iota(jnp.int32, (128, 128), 1).astype(f32)
     for j in range(zs):
         both = jnp.zeros((128, 128), f32)
         for h in range(2):
-            hit = [place + float(j * cap) == r for r in lane_rows[h]]
+            hit = [place + float(j * high) == r for r in lane_rows[h]]
             found = jnp.where(hit[0], slot_of[0], 0.0) + jnp.where(hit[1], slot_of[1], 0.0)
-            found = jnp.broadcast_to(jnp.sum(found, axis=1, keepdims=True) - 1.0, (cap, 128))
+            found = jnp.broadcast_to(jnp.sum(found, axis=1, keepdims=True) - 1.0, (high, 128))
             both = jnp.where(spot == float(h), jnp.concatenate([found, blank], axis=0), both)
         meta[j] = jnp.transpose(both)[0:8, :]
     for o in range(1, zs):
@@ -468,9 +488,9 @@
         for k in range(2):
             row = row_of(columns_ref[:, k : k + 1], columns_ref[:, 2 + k : 3 + k], h)
             weight = weight + jnp.where(row == row_lane, columns_ref[:, 6 + k : 7 + k], 0.0)
-        high = weight.astype(bf)
-        weigh[h, 0] = high
-        weigh[h, 1] = (weight - high.astype(f32)).astype(bf)
+        rounded = weight.astype(bf)
+        weigh[h, 0] = rounded
+        weigh[h, 1] = (weight - rounded.astype(f32)).astype(bf)
     metar[z] = meta[z]
 
     @pl.loop(DEPTH, chunks)
@@ -479,11 +499,11 @@
 
     for o in range(1, zs):
         m_copy(o).wait_recv()
-    places = lax.broadcasted_iota(jnp.int32, (cap, total), 1).astype(f32)
+    places = lax.broadcasted_iota(jnp.int32, (high, total), 1).astype(f32)
     for h in range(2):
         blocks = []
         for j in range(zs):
-            where = jnp.transpose(metar[j])[:cap, h : h + 1]
+            where = jnp.transpose(metar[j])[:high, h : h + 1]
             blocks.append(jnp.where(where == places, one, zero))
         if padded > rows:
             blocks.append(jnp.zeros((padded - rows, total), f32))
@@ -517,10 +537,8 @@
 
         @pl.when(t < chunks)
         def _():
-            sides = unfold(r1, t)
-            for i in range(2):
-                value = dot32(onehot[half_of(t)], sides[i]).astype(bf)
-                s2[t, :, :, i * side : (i + 1) * side] = value.reshape(groups, slots, side)
+            value = dot32(onehot[half_of(t)], unfold(r1, t)).astype(bf)
+            s2[t] = value.reshape(groups, slots, width)
             start_all(g_sends, t, groups)
             r2[t, g_me] = s2[t, g_me]
 
@@ -556,25 +574,24 @@
                 start_all(g_backs, k + DEPTH, groups)
 
             value = dot32(onehot_t[half_of(k)], b2[k].reshape(total, width))
-            o1[k] = fold(value)
+            o1[k] = fold(value[:rows])
             b1[k, z] = o1[k, z]
 
         @pl.when(t >= chunks)
         def _():
             k = t - chunks
             h = half_of(k)
-            sides = unfold(b1, k)
-            for i in range(2):
-                at = pl.ds(pl.multiple_of(lax.rem(k, each) * width + i * side, side), side)
-                value = dot32(weigh[h, 0], sides[i]) + dot32(weigh[h, 1], sides[i])
-
-                @pl.when(h == 0)
-                def _():
-                    partial[:, at] = hidden_ref[:, at].astype(f32) + value
-
-                @pl.when(h == 1)
-                def _():
-                    out_ref[:, at] = (partial[:, at] + value).astype(bf)
+            values = unfold(b1, k)
+            at = columns(k)
+            value = dot32(weigh[h, 0], values) + dot32(weigh[h, 1], values)
+
+            @pl.when(h == 0)
+            def _():
+                partial[:, at] = hidden_ref[:, at].astype(f32) + value
+
+            @pl.when(h == 1)
+            def _():
+                out_ref[:, at] = (partial[:, at] + value).astype(bf)
 
     for o in range(1, zs):
         m_copy(o).wait_send()
@@ -594,12 +611,14 @@
     groups = ys * cs
     tokens, model = normed.shape
     slots = zs * limit // 2
-    padded = -(-zs * cap // 128) * 128
+    high = -(-cap // 8) * 8
+    padded = -(-zs * high // 128) * 128
     chunks = 2 * model // WIDTH
     units = gate.shape[1]
     bf, f32 = jnp.bfloat16, jnp.float32
     vmem, anywhere = pl.BlockSpec(memory_space=pltpu.VMEM), pl.BlockSpec(memory_space=pltpu.HBM)
-    z_block, g_block = (chunks, zs, 2 * cap, WIDTH // 2), (chunks, groups, slots, WIDTH)
+    z_block = (chunks, zs, cap, WIDTH) if high == cap else (chunks, zs, 2 * cap, WIDTH // 2)
+    g_block = (chunks, groups, slots, WIDTH)
     dma = pltpu.SemaphoreType.DMA
     z_sem, g_sem, m_sem = dma((chunks, zs - 1)), dma((chunks, groups - 1)), dma((zs - 1,))
     total = groups * slots
@@ -656,11 +675,11 @@
         expert_ids, group_share, pair_scores, limit,
     )
     arguments = (normed, hidden, columns, lanes, gate_experts[0], up_experts[0], down_experts[0])
-    usual = USUAL
-    return lax.cond(
-        most[0, 0] <= usual,
-        functools.partial(routed_experts, usual, limit, 2),
-        functools.partial(routed_experts, worst, limit, 3),
+    caps = [cap for cap in USUAL if cap < worst]
+    tier = sum((most[0, 0] > cap).astype(jnp.int32) for cap in caps)
+    return lax.switch(
+        tier,
+        [functools.partial(routed_experts, cap, limit, 2 + i) for i, cap in enumerate(caps + [worst])],
         *arguments,
     )
 

time: 179 us -> 169 us (0.944)
  Pallas kernels: 175 us -> 164 us
    pallas_call x1, Pallas kernels: 131 us -> 123 us  [routed_experts(): pl.pallas_call(functools.partial(expert_kernel, zs, ys, cs, cap, slots),...]
    pallas_call x1, Pallas kernels: 43.3 us -> 40.9 us  [mixer(): pl.pallas_call(functools.partial(mixer_kernel, sizes, limit, parts), out_...]
where the time goes in v5:
time: 169 us
  Pallas kernels  164 us (97%)
  local copies, waits for them, and re-layouts  3.28 us (2%)
    pallas_call x1, Pallas kernels, routed_experts(): pl.pallas_call(functools.partial(expert_kernel, zs, ys, cs, cap, slots),...  123 us
    pallas_call x1, Pallas kernels, mixer(): pl.pallas_call(functools.partial(mixer_kernel, sizes, limit, parts), out_...  40.9 us

profile of v5, /device:TPU:1, one launch (start us, length us, event | category | flops | bytes accessed | tf_op | source)
XLA Modules:
  0.0 168.7 jit_solution(1397530857386325733)
XLA Ops:
  0.0 40.9 %mixer.1 = (bf16[192,2048]{1,0:T(8,128)(2,1)}, bf16[192,2048]{1,0:T(8,128)(2,1)}, f32[192,128]{1,0:T(8,128)}, f32[8,256]{1,0:T(8,128)}, f32[8,128]{1,0:T(8,128)}) custom-call(f32[3,512]{1,0:T(4,128)} %taps_hbm.1, f32[1,2048]{1,0:T(1,128)} %bitcast.18, f32[1,2048]{1,0:T(1,128)} %bitcast.19, s32[2,192]{1,0:T(2,128)} %bitcast.20, f32[1,192]{1,0:T(1,128)} %bitcast.22, ...), custom_call_target="tpu_custom_call" | custom-call | tf_op jit(solution)/shard_map/mixer/pallas_call | solution.py:295
  40.9 1.2 slice.4
  43.4 123.2 %conditional.1 = (bf16[192,2048]{1,0:T(8,128)(2,1)}) conditional(s32[]{:T(128)} %bitcast.5, (bf16[192,2048]{1,0:T(8,128)(2,1)}, bf16[192,2048]{1,0:T(8,128)(2,1)}, f32[192,128]{1,0:T(8,128)}, f32[8,256]{1,0:T(8,128)}, bf16[2048,512]{1,0:T(8,128)(2,1)}, /*index=5*/bf16[2048,512]{1,0:T(8,128)(2,1)}, ...), branch_computations={%region_0.0_spmd, %region_1.0_spmd, %region_2.0_spmd} | conditional | bytes 8 | solution.py:680
  43.4 122.9 %routed_experts.3 = bf16[192,2048]{1,0:T(8,128)(2,1)} custom-call(bf16[192,2048]{1,0:T(8,128)(2,1)} %get-tuple-element.50.normed_ref, bf16[192,2048]{1,0:T(8,128)(2,1)} %get-tuple-element.52.hidden_ref, f32[192,128]{1,0:T(8,128)} %get-tuple-element.53.columns_ref, f32[8,256]{1,0:T(8,128)} %get-tuple-element.54.lanes_ref, ...), custom_call_target="tpu_custom_call" | custom-call | tf_op jit(solution)/shard_map/cond/branch_0_fun/routed_experts/pallas_call | solution.py:625
  166.6 2.1 %copy.23 = bf16[192,2048]{1,0:T(8,128)(2,1)} copy(bf16[192,2048]{1,0:T(8,128)(2,1)} %get-tuple-element.82) | data formatting | bytes 1572864

commit v6 on v5

--- a/solution.py
+++ b/solution.py
@@ -16,6 +16,8 @@
 epsilon = 1e-06
 WIDTH = 512
 VMEM_LIMIT = 67043328
+MIXER_ROOM = 1835008
+EXPERT_ROOM = 2726297
 DEPTH = 2
 WINDOW = 3
 USUAL = (36, 40)
@@ -30,10 +32,10 @@
 
 
 def mixer_kernel(
-    sizes, limit, parts,
+    sizes, limit, caps, parts,
     taps_hbm, mix_gain_hbm, expert_gain_hbm, ids_hbm, share_hbm, scores_hbm,
     outer_hbm, inner_hbm, input_hbm, weight_hbm, gate_hbm, residual_hbm,
-    hidden_ref, normed_ref, columns_ref, lanes_ref, most_ref,
+    hidden_ref, normed_ref, columns_ref, lanes_ref, tier_ref,
     taps_ref, mix_gain_ref, expert_gain_ref, ids_v, share_v, scores_v,
     outer_v, inner_v, input_v, weight_v, gate_v, residual_v,
     products, mixed, own, far, far_in, near, near_in, tails, tail_in, table,
@@ -269,7 +271,11 @@
         flag.wait_recv()
     for i in range(zs - 1):
         most = jnp.maximum(most, z_in[i])
-    most_ref[...] = most
+    level = jnp.max(most)
+    tier = jnp.int32(0)
+    for cap in caps:
+        tier = tier + jnp.where(level > cap, 1, 0).astype(jnp.int32)
+    tier_ref[0, 0] = tier
 
     tail_copy.wait_send()
     for h in range(2):
@@ -281,7 +287,7 @@
         flag.wait_send()
 
 
-def mixer(outer, inner, values, taps, weight, gate, residual, mix_gain, expert_gain, ids, share, scores, limit):
+def mixer(outer, inner, values, taps, weight, gate, residual, mix_gain, expert_gain, ids, share, scores, limit, caps):
     sizes = tuple(lax.axis_size(a) for a in SP_TP)
     zs, ys, cs, xs = sizes
     groups = ys * cs
@@ -293,16 +299,16 @@
     dma = pltpu.SemaphoreType.DMA
     flag = (8, 128)
     return pl.pallas_call(
-        functools.partial(mixer_kernel, sizes, limit, parts),
+        functools.partial(mixer_kernel, sizes, limit, caps, parts),
         out_shape=(
             jax.ShapeDtypeStruct((rows, model), bf),
             jax.ShapeDtypeStruct((rows, model), bf),
             jax.ShapeDtypeStruct((rows, 128), f32),
             jax.ShapeDtypeStruct((8, 256), f32),
-            jax.ShapeDtypeStruct(flag, f32),
+            jax.ShapeDtypeStruct((1, 1), jnp.int32),
         ),
         in_specs=[anywhere] * 12,
-        out_specs=(vmem,) * 5,
+        out_specs=(vmem,) * 4 + (pl.BlockSpec(memory_space=pltpu.SMEM),),
         scratch_shapes=[
             pltpu.VMEM(taps.shape, f32), pltpu.VMEM((1, model), f32), pltpu.VMEM((1, model), f32),
             pltpu.VMEM((2, rows), jnp.int32), pltpu.VMEM((1, rows), f32), pltpu.VMEM((2, rows), f32),
@@ -323,7 +329,7 @@
             dma((xs - 1,)), dma((xs - 1,)), dma((groups - 1,)), dma((groups - 1,)), dma((zs - 1,)), dma((zs - 1,)),
         ],
         compiler_params=pltpu.CompilerParams(
-            collective_id=1, has_side_effects=True, vmem_limit_bytes=VMEM_LIMIT
+            collective_id=1, has_side_effects=True, vmem_limit_bytes=VMEM_LIMIT - MIXER_ROOM
         ),
         name="mixer",
     )(
@@ -347,7 +353,9 @@
     each = chunks // 2
     high = -(-cap // 8) * 8
     width = s2.shape[3]
-    side = width // 2
+    odd = cap % 8
+    folds = 8 // odd if odd else 1
+    side, whole = width // folds, cap - odd
     tokens = normed_ref.shape[0]
     rows = zs * high
     padded = onehot_t.shape[1]
@@ -419,28 +427,30 @@
 
     def fold(value):
         value = value.reshape(zs, high, width)
-        if high == cap:
+        if folds == 1:
             return value.astype(bf)
-        whole = high - 8
-        left, right = value[:, :, :side], value[:, :, side:]
         blocks = []
         for j in range(zs):
-            ends = left[j, whole:] + pltpu.roll(right[j, whole:], 4, 0)
-            blocks.append(jnp.concatenate([left[j, :whole], right[j, :whole], ends], axis=0)[None])
+            sides = [value[j, :, i * side : (i + 1) * side] for i in range(folds)]
+            ends = sides[0][whole:]
+            for i in range(1, folds):
+                ends = ends + pltpu.roll(sides[i][whole:], i * odd, 0)
+            blocks.append(jnp.concatenate([v[:whole] for v in sides] + [ends], axis=0)[None])
         return jnp.concatenate(blocks, axis=0).astype(bf)
 
     def unfold(ref, k):
         value = ref[k].astype(f32)
-        if high == cap:
+        if folds == 1:
             blocks = [value.reshape(rows, width)]
         else:
-            whole = high - 8
             blocks = []
             for j in range(zs):
-                ends = value[j, 2 * whole :]
-                left = jnp.concatenate([value[j, :whole], ends], axis=0)
-                right = jnp.concatenate([value[j, whole : 2 * whole], pltpu.roll(ends, 4, 0)], axis=0)
-                blocks.append(jnp.concatenate([left, right], axis=1))
+                ends = value[j, folds * whole :]
+                sides = []
+                for i in range(folds):
+                    end = pltpu.roll(ends, 8 - i * odd, 0) if i else ends
+                    sides.append(jnp.concatenate([value[j, i * whole : (i + 1) * whole], end], axis=0))
+                blocks.append(jnp.concatenate(sides, axis=1))
         if padded > rows:
             blocks.append(jnp.zeros((padded - rows, width), f32))
         return jnp.concatenate(blocks, axis=0).astype(bf)
@@ -531,9 +541,19 @@
         def _():
             start_all(z_sends, t + DEPTH, zs)
 
-        @pl.when((t + DEPTH >= chunks) & (t + DEPTH < 2 * chunks))
+        @pl.when((t > each) & (t <= each + chunks))
         def _():
-            start_all(z_backs, t + DEPTH - chunks, zs)
+            k = t - each - 1
+            wait_recv_all(g_backs, k, groups)
+
+            @pl.when(lax.rem(k, each) + DEPTH < each)
+            def _():
+                start_all(g_backs, k + DEPTH, groups)
+
+            value = dot32(onehot_t[half_of(k)], b2[k].reshape(total, width))
+            o1[k] = fold(value[:rows])
+            b1[k, z] = o1[k, z]
+            start_all(z_backs, k, zs)
 
         @pl.when(t < chunks)
         def _():
@@ -564,19 +584,6 @@
                 if i < DEPTH:
                     start_all(g_backs, k, groups)
 
-        @pl.when((t > each) & (t <= each + chunks))
-        def _():
-            k = t - each - 1
-            wait_recv_all(g_backs, k, groups)
-
-            @pl.when(lax.rem(k, each) + DEPTH < each)
-            def _():
-                start_all(g_backs, k + DEPTH, groups)
-
-            value = dot32(onehot_t[half_of(k)], b2[k].reshape(total, width))
-            o1[k] = fold(value[:rows])
-            b1[k, z] = o1[k, z]
-
         @pl.when(t >= chunks)
         def _():
             k = t - chunks
@@ -617,7 +624,8 @@
     units = gate.shape[1]
     bf, f32 = jnp.bfloat16, jnp.float32
     vmem, anywhere = pl.BlockSpec(memory_space=pltpu.VMEM), pl.BlockSpec(memory_space=pltpu.HBM)
-    z_block = (chunks, zs, cap, WIDTH) if high == cap else (chunks, zs, 2 * cap, WIDTH // 2)
+    folds = 8 // (cap % 8) if cap % 8 else 1
+    z_block = (chunks, zs, folds * cap, WIDTH // folds)
     g_block = (chunks, groups, slots, WIDTH)
     dma = pltpu.SemaphoreType.DMA
     z_sem, g_sem, m_sem = dma((chunks, zs - 1)), dma((chunks, groups - 1)), dma((zs - 1,))
@@ -645,7 +653,7 @@
             dma((3,)),
         ],
         compiler_params=pltpu.CompilerParams(
-            collective_id=collective, has_side_effects=True, vmem_limit_bytes=VMEM_LIMIT
+            collective_id=collective, has_side_effects=True, vmem_limit_bytes=VMEM_LIMIT - EXPERT_ROOM
         ),
         name="routed_experts",
     )(normed, hidden, columns, lanes, gate, up, down)
@@ -670,15 +678,14 @@
 ):
     limit = 2 * expert_ids.shape[1] * residual.shape[0] // (lax.axis_size(SP) * gate_experts.shape[0])
     worst = limit * lax.axis_size(Y) * lax.axis_size(CORE) // 2
-    hidden, normed, columns, lanes, most = mixer(
+    caps = [cap for cap in USUAL if cap < worst]
+    hidden, normed, columns, lanes, tier = mixer(
         conv_outer, conv_inner, conv_input, conv_taps, out_weight, mix_gate, residual, mix_gain, expert_gain,
-        expert_ids, group_share, pair_scores, limit,
+        expert_ids, group_share, pair_scores, limit, caps,
     )
     arguments = (normed, hidden, columns, lanes, gate_experts[0], up_experts[0], down_experts[0])
-    caps = [cap for cap in USUAL if cap < worst]
-    tier = sum((most[0, 0] > cap).astype(jnp.int32) for cap in caps)
     return lax.switch(
-        tier,
+        tier[0, 0],
         [functools.partial(routed_experts, cap, limit, 2 + i) for i, cap in enumerate(caps + [worst])],
         *arguments,
     )

time: 169 us -> 162 us (0.959)
  Pallas kernels: 164 us -> 160 us
  local copies, waits for them, and re-layouts: 3.28 us -> 0.88 us
    pallas_call x1, Pallas kernels: 123 us -> 119 us  [routed_experts(): pl.pallas_call(functools.partial(expert_kernel, zs, ys, cs, cap, slots),...]
where the time goes in v6:
time: 162 us
  Pallas kernels  160 us (99%)
    pallas_call x1, Pallas kernels, routed_experts(): pl.pallas_call(functools.partial(expert_kernel, zs, ys, cs, cap, slots),...  119 us
    pallas_call x1, Pallas kernels, mixer(): pl.pallas_call(functools.partial(mixer_kernel, sizes, limit, caps, parts)...  40.4 us

profile of v6, /device:TPU:1, one launch (start us, length us, event | category | flops | bytes accessed | tf_op | source)
XLA Modules:
  0.0 161.5 jit_solution(18093741158654308203)
XLA Ops:
  0.0 40.4 %mixer.1 = (bf16[192,2048]{1,0:T(8,128)(2,1)S(1)}, bf16[192,2048]{1,0:T(8,128)(2,1)S(1)}, f32[192,128]{1,0:T(8,128)S(1)}, f32[8,256]{1,0:T(8,128)S(1)}, s32[1,1]{1,0:T(1,128)}) custom-call(f32[3,512]{1,0:T(4,128)} %taps_hbm.1, f32[1,2048]{1,0:T(1,128)} %bitcast.18, f32[1,2048]{1,0:T(1,128)} %bitcast.19, s32[2,192]{1,0:T(2,128)} %bitcast.20, ...), custom_call_target="tpu_custom_call" | custom-call | tf_op jit(solution)/shard_map/mixer/pallas_call | solution.py:301
  41.0 119.6 %conditional.1 = (bf16[192,2048]{1,0:T(8,128)(2,1)S(1)}) conditional(s32[]{:T(128)} %bitcast.5, (bf16[192,2048]{1,0:T(8,128)(2,1)S(1)}, bf16[192,2048]{1,0:T(8,128)(2,1)S(1)}, f32[192,128]{1,0:T(8,128)S(1)}, f32[8,256]{1,0:T(8,128)S(1)}, bf16[2048,512]{1,0:T(8,128)(2,1)}, /*index=5*/bf16[2048,512]{1,0:T(8,128)(2,1)}, ...), branch_computations={%region_0.0_spmd, %region_1.0_spmd, %region_2.0_spmd} | conditional | bytes 8 | solution.py:687
  41.0 119.4 %routed_experts.3 = bf16[192,2048]{1,0:T(8,128)(2,1)S(1)} custom-call(bf16[192,2048]{1,0:T(8,128)(2,1)S(1)} %get-tuple-element.50.normed_ref, bf16[192,2048]{1,0:T(8,128)(2,1)S(1)} %get-tuple-element.52.hidden_ref, f32[192,128]{1,0:T(8,128)S(1)} %get-tuple-element.53.columns_ref, f32[8,256]{1,0:T(8,128)S(1)} %get-tuple-element.54.lanes_ref, ...), custom_call_target="tpu_custom_call" | custom-call | tf_op jit(solution)/shard_map/cond/branch_0_fun/routed_experts/pallas_call | solution.py:633
  160.6 0.9 copy.23
